TPU v7x, 32 devices: a whole 2x2x4 slice. The times are simulated.
32 devices in a mesh: sp: 16 (over z, y, x), tp: 2 (over core).
Axes of the slice: x: 2, y: 2, z: 4, core: 2. Of those that a mesh axis runs over, the one named last changes fastest.
Arguments:
- mixer_output: bfloat16 [2048, 2048], P('sp'), may hold values from -6 to 6
- layer_cotangent: bfloat16 [2048, 2048], P('sp'), may hold values from -6 to 6
- expert_choice: int32 [2048, 2], P('sp'), may hold values from 0 to 15, all different within a row; in each aligned block of 128 rows (0 to 127, 128 to 255, ...) at most 32 rows name the same one
- route_weight: float32 [2048, 2], P('sp'), may hold values from 0.1 to 0.9
- gate_pre: bfloat16 [16, 512, 1024], P('sp', None, 'tp'), may hold values from -15 to 15
- up_pre: bfloat16 [16, 512, 1024], P('sp', None, 'tp'), may hold values from -15 to 15
- w_gate: bfloat16 [16, 2048, 1024], P('sp', None, 'tp'), may hold values from -0.125 to 0.125
- w_up: bfloat16 [16, 2048, 1024], P('sp', None, 'tp'), may hold values from -0.125 to 0.125
- w_down: bfloat16 [16, 1024, 2048], P('sp', 'tp'), may hold values from -0.1875 to 0.1875
- w_out: bfloat16 [2048, 2048], P('tp'), may hold values from -0.125 to 0.125
- norm_gain: bfloat16 [2048], P('tp'), may hold values from 0.099609375 to 1.8984375
- scan_in: bfloat16 [2048, 2048], P('sp', 'tp'), may hold values from -6 to 6
- gate_in: bfloat16 [2048, 2048], P('sp', 'tp'), may hold values from -9 to 9
- b_proj: bfloat16 [2048, 1024], P('sp', 'tp'), may hold values from -1.796875 to 1.796875
- c_proj: bfloat16 [2048, 1024], P('sp', 'tp'), may hold values from -1.796875 to 1.796875
- log_decay: float32 [2048, 32], P('sp', 'tp'), may hold values from -3 to 0
- entry_state: float32 [16, 32, 64, 128], P('sp', 'tp'), may hold values from -24 to 24
Outputs:
- grad_w_gate: bfloat16 [16, 2048, 1024], P('sp', None, 'tp')
- grad_w_up: bfloat16 [16, 2048, 1024], P('sp', None, 'tp')
- grad_w_down: bfloat16 [16, 1024, 2048], P('sp', 'tp')
- grad_out_proj: float32 [2048, 2048], P('sp', 'tp')
- grad_scan_in: bfloat16 [2048, 2048], P('sp', 'tp')
- grad_gate_in: bfloat16 [2048, 2048], P('sp', 'tp')
- grad_b_proj: bfloat16 [2048, 1024], P('sp', 'tp')
- grad_c_proj: bfloat16 [2048, 1024], P('sp', 'tp')
- grad_log_decay: float32 [2048, 32], P('sp', 'tp')
Inputs may be any that keep to these rules, and one draw needn't show every extreme that they name: `expert_choice`: in the 128 rows of one device no expert is named more than 32 times, a bound that some blocks reach; the 2 entries of a row differ.
All inputs are finite; a program needn't handle non-finite values.
Results may differ from a plain program's by a relative error of at most 0.012.
Values may be sent and summed in bfloat16 or wider, within the bound.
A program may use at most 192 MiB of HBM per device.

v0:
```python
import jax
import jax.numpy as jnp
from jax import lax
from jax.sharding import PartitionSpec as P

HEAD_DIM = 64
STATE = 128


rms_epsilon = 1e-05
clamp_limit = 7.0
swish_alpha = 1.702


def entry_slots(expert_choice, expert_count, capacity):
    tokens, top_count = expert_choice.shape
    targets = expert_choice.reshape(-1)
    experts = jnp.arange(expert_count, dtype=jnp.int32)
    one_hot = (targets[:, None] == experts[None, :]).astype(jnp.float32)
    entries = jnp.arange(tokens * top_count, dtype=jnp.int32)
    before = (entries[:, None] > entries[None, :]).astype(jnp.bfloat16)
    earlier = jnp.dot(before, one_hot.astype(jnp.bfloat16), preferred_element_type=jnp.float32)
    ranks = jnp.sum(earlier * one_hot, axis=1).astype(jnp.int32)
    return (targets * capacity + ranks).reshape(tokens, top_count)


def expert_side(grad_rows, gate_value, up_value, gate_weight, up_weight, down_weight):
    act_grad = jnp.einsum("rd,fd->rf", grad_rows, down_weight, preferred_element_type=jnp.float32)
    gate_full = gate_value.astype(jnp.float32)
    up_full = up_value.astype(jnp.float32)
    gate_clip = jnp.minimum(gate_full, clamp_limit)
    up_clip = jnp.clip(up_full, -clamp_limit, clamp_limit)
    sigmoid_gate = jax.nn.sigmoid(swish_alpha * gate_clip)
    swish_gate = gate_clip * sigmoid_gate
    active = ((up_clip + 1.0) * swish_gate).astype(jnp.bfloat16)
    up_grad = jnp.where(
        (up_full > -clamp_limit) & (up_full < clamp_limit), act_grad * swish_gate, 0.0
    ).astype(jnp.bfloat16)
    slope = sigmoid_gate + swish_alpha * gate_clip * sigmoid_gate * (1.0 - sigmoid_gate)
    gate_grad = jnp.where(gate_full < clamp_limit, act_grad * (up_clip + 1.0) * slope, 0.0).astype(
        jnp.bfloat16
    )
    partial_rows = jnp.einsum(
        "rf,df->rd", gate_grad, gate_weight, preferred_element_type=jnp.float32
    )
    partial_rows = partial_rows + jnp.einsum(
        "rf,df->rd", up_grad, up_weight, preferred_element_type=jnp.float32
    )
    return (active, gate_grad, up_grad, partial_rows)


def exchange(pieces):
    return lax.all_to_all(pieces, "sp", split_axis=0, concat_axis=0, tiled=True)


def tell_all(vector):
    return exchange(jnp.broadcast_to(vector, (lax.axis_size("sp"), *vector.shape)))


def later_states(block_state, totals):
    count = lax.axis_size("sp")
    heads, channels, width = block_state.shape
    rows = heads * channels // count
    spots = jnp.arange(count)
    between = (
        (spots[:, None, None] < spots[None, None, :]) & (spots[None, None, :] < spots[None, :, None])
    ).astype(jnp.float32)
    gaps = jnp.einsum("bck,kh->bch", between, totals, precision=lax.Precision.HIGHEST)
    later = spots[:, None, None] < spots[None, :, None]
    weights = jnp.where(later, jnp.exp(gaps), 0.0)
    first = lax.axis_index("sp") * rows
    picks = (
        ((first + jnp.arange(rows)) // channels)[None, :] == jnp.arange(heads)[:, None]
    ).astype(jnp.float32)
    weights = jnp.einsum("bch,hr->bcr", weights, picks, precision=lax.Precision.HIGHEST)
    dealt = lax.all_to_all(
        block_state.astype(jnp.bfloat16).reshape(count, rows, width),
        "sp",
        split_axis=0,
        concat_axis=0,
        tiled=True,
    ).astype(jnp.float32)
    sums = jnp.sum(weights[:, :, :, None] * dealt[None], axis=1)
    back = lax.all_to_all(
        sums.astype(jnp.bfloat16), "sp", split_axis=0, concat_axis=0, tiled=True
    )
    return back.reshape(heads, channels, width)


def body(
    mixer_output,
    layer_cotangent,
    expert_choice,
    route_weight,
    gate_pre,
    up_pre,
    w_gate,
    w_up,
    w_down,
    w_out,
    norm_gain,
    scan_in,
    gate_in,
    b_proj,
    c_proj,
    log_decay,
    entry_state,
):
    expert_count = lax.axis_size("sp")
    tokens_here = mixer_output.shape[0]
    model_width = mixer_output.shape[1]
    top_count = expert_choice.shape[1]
    capacity = gate_pre.shape[1] // expert_count
    columns = model_width // lax.axis_size("tp")
    first_column = lax.axis_index("tp") * columns
    own_cotangent = lax.dynamic_slice_in_dim(layer_cotangent, first_column, columns, 1).astype(
        jnp.float32
    )
    own_hidden = lax.dynamic_slice_in_dim(mixer_output, first_column, columns, 1)
    slots = entry_slots(expert_choice, expert_count, capacity)
    slot_ids = jnp.arange(expert_count * capacity, dtype=jnp.int32)
    places = (slots.T[:, None, :] == slot_ids[None, :, None]).astype(jnp.bfloat16)
    token_places = places.sum(axis=0)
    weighted = (route_weight.T[:, :, None] * own_cotangent[None]).astype(jnp.bfloat16)

    def dispatch(rows):
        arrived = lax.all_to_all(
            rows.astype(jnp.bfloat16).reshape(expert_count, capacity, columns),
            "sp",
            split_axis=0,
            concat_axis=0,
            tiled=True,
        ).reshape(-1, columns)
        return lax.all_gather(arrived, "tp", axis=1, tiled=True)

    recv_grads = dispatch(
        jnp.einsum("kst,ktd->sd", places, weighted, preferred_element_type=jnp.float32)
    )
    active, gate_grad, up_grad, partial_rows = expert_side(
        recv_grads,
        gate_pre[0],
        up_pre[0],
        w_gate[0],
        w_up[0],
        w_down[0],
    )
    summed = lax.psum_scatter(
        partial_rows.astype(jnp.bfloat16), "tp", scatter_dimension=1, tiled=True
    )
    returned = lax.all_to_all(
        summed.reshape(expert_count, capacity, -1), "sp", split_axis=0, concat_axis=0, tiled=True
    )
    head_count = log_decay.shape[1]
    group_count = b_proj.shape[1] // STATE
    per_group = head_count // group_count
    scan_heads = scan_in.reshape(tokens_here, head_count, HEAD_DIM)
    b_groups = b_proj.reshape(tokens_here, group_count, STATE)
    c_groups = c_proj.reshape(tokens_here, group_count, STATE)
    x_float = scan_heads.astype(jnp.float32)
    token_locations = jnp.arange(tokens_here)
    causal = token_locations[:, None] >= token_locations[None, :]
    causal_float = causal.astype(jnp.float32)
    cumulative = jnp.dot(causal_float, log_decay, precision=lax.Precision.HIGHEST)
    growth = jnp.exp(cumulative)
    block_decays = tell_all(lax.optimization_barrier((cumulative[-1], summed))[0])
    tail_decay = jnp.exp(cumulative[-1][None, :] - cumulative)
    log_gaps = cumulative.T[:, :, None] - cumulative.T[:, None, :]
    decay_mat = jnp.exp(jnp.where(causal[None], log_gaps, -jnp.inf))
    inner_prod = jnp.einsum("tgn,sgn->gts", c_groups, b_groups, preferred_element_type=jnp.float32)
    mix_weights = (jnp.repeat(inner_prod, per_group, axis=0) * decay_mat).astype(jnp.bfloat16)
    state_groups = entry_state.astype(jnp.bfloat16).reshape(group_count, per_group, HEAD_DIM, STATE)
    y_inner = jnp.einsum(
        "hts,shp->thp", mix_weights, scan_heads, preferred_element_type=jnp.float32
    )
    y_carry = jnp.einsum(
        "tgn,grpn->tgrp", c_groups, state_groups, preferred_element_type=jnp.float32
    ).reshape(tokens_here, head_count, HEAD_DIM)
    scan_out = y_inner + y_carry * growth[:, :, None]
    gate_float = gate_in.astype(jnp.float32)
    gate_sig = jax.nn.sigmoid(gate_float)
    gate_silu = gate_float * gate_sig
    gated = scan_out.reshape(tokens_here, -1) * gate_silu
    grouped = gated.reshape(tokens_here, group_count, -1)
    inv_rms = lax.rsqrt(jnp.mean(grouped * grouped, axis=-1, keepdims=True) + rms_epsilon)
    unit = grouped * inv_rms
    gain_groups = norm_gain.astype(jnp.float32).reshape(group_count, -1)
    mixed = (unit * gain_groups).reshape(tokens_here, -1).astype(jnp.bfloat16)
    all_mixed = lax.all_gather(mixed, "sp", axis=0, tiled=True)
    returned, mixed = lax.optimization_barrier((returned, mixed))
    moe_terms = jnp.einsum(
        "st,sd->td",
        token_places,
        returned.reshape(-1, columns),
        preferred_element_type=jnp.float32,
    )
    grad_hidden = lax.all_gather(
        (own_cotangent + moe_terms).astype(jnp.bfloat16), "tp", axis=1, tiled=True
    )
    late_hidden, grad_hidden = lax.optimization_barrier((own_hidden, grad_hidden))
    recv_hidden = dispatch(
        jnp.einsum("st,td->sd", token_places, late_hidden, preferred_element_type=jnp.float32)
    )
    down_wgrad = jnp.einsum(
        "rf,rd->fd", active, recv_grads, preferred_element_type=jnp.float32
    ).astype(jnp.bfloat16)
    gate_wgrad = jnp.einsum(
        "rd,rf->df", recv_hidden, gate_grad, preferred_element_type=jnp.float32
    ).astype(jnp.bfloat16)
    up_wgrad = jnp.einsum(
        "rd,rf->df", recv_hidden, up_grad, preferred_element_type=jnp.float32
    ).astype(jnp.bfloat16)
    own_block = lax.all_to_all(
        grad_hidden.reshape(tokens_here, expert_count, -1).transpose(1, 0, 2),
        "sp",
        split_axis=0,
        concat_axis=0,
        tiled=True,
    )
    grad_out_proj = jnp.einsum(
        "td,ti->di",
        own_block.reshape(-1, own_block.shape[2]),
        all_mixed,
        preferred_element_type=jnp.float32,
    )
    grad_mixed = jnp.einsum("td,id->ti", grad_hidden, w_out, preferred_element_type=jnp.float32)
    grad_unit = grad_mixed.reshape(tokens_here, group_count, -1) * gain_groups
    grad_grouped = inv_rms * (grad_unit - unit * jnp.mean(grad_unit * unit, axis=-1, keepdims=True))
    grad_gated = grad_grouped.reshape(tokens_here, -1)
    grad_gate_in = (
        grad_gated
        * scan_out.reshape(tokens_here, -1)
        * gate_sig
        * (1.0 + gate_float * (1.0 - gate_sig))
    ).astype(jnp.bfloat16)
    grad_y = (grad_gated * gate_silu).reshape(tokens_here, head_count, HEAD_DIM)
    grad_y_b = grad_y.astype(jnp.bfloat16)
    grad_x_inner = jnp.einsum(
        "hts,thp->shp", mix_weights, grad_y_b, preferred_element_type=jnp.float32
    )
    grad_weights = (
        jnp.einsum("thp,shp->hts", grad_y_b, scan_heads, preferred_element_type=jnp.float32)
        * decay_mat
    )
    grad_weights = (
        grad_weights.reshape(group_count, per_group, tokens_here, tokens_here)
        .sum(axis=1)
        .astype(jnp.bfloat16)
    )
    grad_c_inner = jnp.einsum(
        "gts,sgn->tgn", grad_weights, b_groups, preferred_element_type=jnp.float32
    )
    grad_b_inner = jnp.einsum(
        "gts,tgn->sgn", grad_weights, c_groups, preferred_element_type=jnp.float32
    )
    grown_grads = (grad_y * growth[:, :, None]).astype(jnp.bfloat16).reshape(
        tokens_here, group_count, per_group, HEAD_DIM
    )
    grad_c_carry = jnp.einsum(
        "tgrp,grpn->tgn", grown_grads, state_groups, preferred_element_type=jnp.float32
    )
    block_state = jnp.einsum(
        "tgrp,tgn->grpn", grown_grads, c_groups, preferred_element_type=jnp.float32
    ).reshape(head_count, HEAD_DIM, STATE)
    x_tail = (x_float * tail_decay[:, :, None]).astype(jnp.bfloat16).reshape(
        tokens_here, group_count, per_group, HEAD_DIM
    )
    later_state = later_states(block_state, block_decays)
    later_groups = later_state.reshape(group_count, per_group, HEAD_DIM, STATE)
    grad_x_carry = jnp.einsum(
        "sgn,grpn->sgrp", b_groups, later_groups, preferred_element_type=jnp.float32
    ).reshape(tokens_here, head_count, HEAD_DIM)
    grad_x = grad_x_inner + grad_x_carry * tail_decay[:, :, None]
    grad_b_carry = jnp.einsum(
        "sgrp,grpn->sgn", x_tail, later_groups, preferred_element_type=jnp.float32
    )
    grad_a = jnp.sum(grad_y * scan_out, axis=2) - jnp.sum(x_float * grad_x, axis=2)
    block_totals = tell_all(jnp.sum(grad_a, axis=0))
    is_later = jnp.arange(expert_count) > lax.axis_index("sp")
    later_grad = jnp.sum(jnp.where(is_later[:, None], block_totals, 0.0), axis=0)
    grad_log_decay = (
        jnp.dot(causal_float.T, grad_a, precision=lax.Precision.HIGHEST) + later_grad[None, :]
    )
    grad_scan_in = grad_x.reshape(tokens_here, -1).astype(jnp.bfloat16)
    grad_b_proj = (grad_b_inner + grad_b_carry).reshape(tokens_here, -1).astype(jnp.bfloat16)
    grad_c_proj = (grad_c_inner + grad_c_carry).reshape(tokens_here, -1).astype(jnp.bfloat16)
    return (
        gate_wgrad[None],
        up_wgrad[None],
        down_wgrad[None],
        grad_out_proj,
        grad_scan_in,
        grad_gate_in,
        grad_b_proj,
        grad_c_proj,
        grad_log_decay,
    )


def solution(mesh):
    in_specs = (
        P("sp", None),
        P("sp", None),
        P("sp", None),
        P("sp", None),
        P("sp", None, "tp"),
        P("sp", None, "tp"),
        P("sp", None, "tp"),
        P("sp", None, "tp"),
        P("sp", "tp", None),
        P("tp", None),
        P("tp"),
        P("sp", "tp"),
        P("sp", "tp"),
        P("sp", "tp"),
        P("sp", "tp"),
        P("sp", "tp"),
        P("sp", "tp", None, None),
    )
    out_specs = (
        P("sp", None, "tp"),
        P("sp", None, "tp"),
        P("sp", "tp", None),
        P("sp", "tp"),
        P("sp", "tp"),
        P("sp", "tp"),
        P("sp", "tp"),
        P("sp", "tp"),
        P("sp", "tp"),
    )
    return jax.shard_map(body, mesh=mesh, in_specs=in_specs, out_specs=out_specs, check_vma=False)
```

profile of v0, /device:TPU:0, one launch (start us, length us, event | category | flops | bytes accessed | tf_op | source)
XLA Modules:
  0.0 248.3 jit_solution(7997684214962049168)
XLA Ops:
  11.3 1.3 bitcast_convert_fusion
  12.6 34.6 %all_to_all.48 = bf16[16,32,1024]{2,1,0:T(8,128)(2,1)} all-to-all(bf16[16,32,1024]{2,1,0:T(8,128)(2,1)S(1)} %bitcast.204), channel_id=1, replica_groups=mesh['sp'=16,'tp'=2] {'sp'}, dimensions={0} | all-to-all | bytes 2097152 | tf_op jit(solution)/shard_map/all_to_all | solution.py:127
  47.2 9.0 %all-gather.4.cloned.1.call-done = bf16[512,2048]{1,0:T(8,128)(2,1)} async-done(((bf16[512,1024]{1,0:T(8,128)(2,1)}), bf16[512,2048]{1,0:T(8,128)(2,1)}) %all-gather.4.cloned.1.call-update) | async-done | bytes 2097168 | tf_op jit(solution)/shard_map/all_gather | solution.py:134
  56.2 3.8 %select_convert_fusion = (bf16[512,512]{1,0:T(8,128)(2,1)S(1)}, f32[512,512]{1,0:T(8,128)S(1)}) fusion(bf16[1,512,512]{2,1,0:T(8,128)(2,1)S(1)} %copy-done.42, bf16[1,512,512]{2,1,0:T(8,128)(2,1)S(1)} %copy-done.40, bf16[512,2048]{1,0:T(8,128)(2,1)} %all-gather.4.cloned.1.call-done, bf16[1,512,2048]{2,1,0:T(8,128)(2,1)} %param.25), kind=kOutput, calls=%fused_computation.62 | convolution fusion | flops 1077411840 | bytes 6815744 | tf_op jit(solution)/shard_map/rd,fd->rf/dot_general | solution.py:28
  60.1 1.7 fusion.4
  62.3 2.6 %add_convert_fusion = bf16[512,2048]{1,0:T(8,128)(2,1)} fusion(f32[512,2048]{1,0:T(8,128)S(1)} %fusion.4, bf16[512,512]{1,0:T(8,128)(2,1)S(1)} %get-tuple-element.79, bf16[1,2048,512]{2,1,0:T(8,128)(2,1)S(1)} %copy-done.11), kind=kOutput, calls=%fused_computation.1 | convolution fusion | flops 1075838976 | bytes 8912896 | tf_op jit(solution)/shard_map/rf,df->rd/dot_general | solution.py:46
  69.1 1.0 copy.132
  70.1 1.3 fusion.58
  71.4 1.0 reshape.248
  72.4 1.3 multiply_reduce_fusion.4
  74.4 1.1 multiply_convert_fusion.3
  75.9 7.0 %all-to-all-start.1 = ((bf16[16,32,1024]{2,1,0:T(8,128)(2,1)}), bf16[16,32,1024]{2,1,0:T(8,128)(2,1)}, u32[]{:S(2)}, u32[]{:S(2)}) async-start(bf16[16,32,1024]{2,1,0:T(8,128)(2,1)} %bitcast.217), calls=%async_computation.2 | async-start | bytes 2097152 | tf_op jit(solution)/shard_map/all_to_all | solution.py:150
  83.5 1.7 constant_dynamic-slice_fusion
  85.2 27.8 %all-to-all-done.1 = bf16[16,32,1024]{2,1,0:T(8,128)(2,1)} async-done(((bf16[16,32,1024]{2,1,0:T(8,128)(2,1)}), bf16[16,32,1024]{2,1,0:T(8,128)(2,1)}, u32[]{:S(2)}, u32[]{:S(2)}) %all-to-all-start.1) | async-done | bytes 1048608 | tf_op jit(solution)/shard_map/all_to_all | solution.py:150
  113.7 6.2 %all-to-all-start.4 = ((f32[16,1,16]{2,1,0:T(1,128)}), f32[16,1,16]{2,1,0:T(1,128)}, u32[]{:S(2)}, u32[]{:S(2)}) async-start(f32[16,1,16]{2,1,0:T(1,128)} %broadcast_in_dim.61), calls=%async_computation.5 | async-start | bytes 16384 | tf_op jit(solution)/shard_map/all_to_all | solution.py:53
  119.9 1.6 fusion.10
  121.5 2.2 all_gather.13
  124.5 4.5 %fusion.86 = f32[128,1024]{1,0:T(8,128)} fusion(bf16[128,2048]{1,0:T(8,128)(2,1)S(1)} %all_gather.13, bf16[1024,2048]{1,0:T(8,128)(2,1)} %param.26), kind=kOutput, calls=%fused_computation.145 | convolution fusion | flops 536870912 | bytes 5242880 | tf_op jit(solution)/shard_map/td,id->ti/dot_general | solution.py:225
  129.0 2.1 reshape.254
  131.2 1.7 multiply_reduce_fusion.3
  133.3 1.0 fusion.43
  135.2 1.2 copy.134
  137.4 6.9 %all-to-all-start.5 = ((bf16[16,64,128]{2,1,0:T(8,128)(2,1)}), bf16[16,64,128]{2,1,0:T(8,128)(2,1)}, u32[]{:S(2)}, u32[]{:S(2)}) async-start(bf16[16,64,128]{2,1,0:T(8,128)(2,1)} %bitcast.216), calls=%async_computation.6 | async-start | bytes 524288 | tf_op jit(solution)/shard_map/all_to_all | solution.py:76
  144.3 2.4 convolution_convert_fusion.3
  146.7 12.2 %all-to-all-done.5 = bf16[16,64,128]{2,1,0:T(8,128)(2,1)} async-done(((bf16[16,64,128]{2,1,0:T(8,128)(2,1)}), bf16[16,64,128]{2,1,0:T(8,128)(2,1)}, u32[]{:S(2)}, u32[]{:S(2)}) %all-to-all-start.5) | async-done | bytes 262176 | tf_op jit(solution)/shard_map/all_to_all | solution.py:76
  158.9 7.2 %all-to-all-start.2 = ((bf16[16,32,1024]{2,1,0:T(8,128)(2,1)}), bf16[16,32,1024]{2,1,0:T(8,128)(2,1)}, u32[]{:S(2)}, u32[]{:S(2)}) async-start(bf16[16,32,1024]{2,1,0:T(8,128)(2,1)} %bitcast.202), calls=%async_computation.3 | async-start | bytes 2097152 | tf_op jit(solution)/shard_map/all_to_all | solution.py:127
  166.6 4.8 %fusion.2 = bf16[1,512,2048]{2,1,0:T(8,128)(2,1)} fusion(bf16[512,2048]{1,0:T(8,128)(2,1)} %all-gather.4.cloned.1.call-done, bf16[1,512,512]{2,1,0:T(8,128)(2,1)} %param.22, bf16[1,512,512]{2,1,0:T(8,128)(2,1)} %param.21), kind=kOutput, calls=%fused_computation.7 | convolution fusion | flops 1077936128 | bytes 5242880 | tf_op jit(solution)/shard_map/rf,rd->fd/dot_general | solution.py:203
  172.6 1.0 convolution_bitcast_fusion.2
  173.6 1.2 bitcast_reduce_fusion
  175.7 3.3 %multiply_reduce_fusion = bf16[16,64,128]{2,1,0:T(8,128)(2,1)} fusion(f32[16,64,128]{2,1,0:T(8,128)S(1)} %convert_element_type.168, f32[16,16,64]{2,1,0:T(8,128)S(1)} %fusion.74), kind=kLoop, calls=%fused_computation | loop fusion | flops 4063232 | bytes 851968 | tf_op jit(solution)/shard_map/reduce_sum | solution.py:83
  179.0 10.2 %all-to-all-done.2 = bf16[16,32,1024]{2,1,0:T(8,128)(2,1)} async-done(((bf16[16,32,1024]{2,1,0:T(8,128)(2,1)}), bf16[16,32,1024]{2,1,0:T(8,128)(2,1)}, u32[]{:S(2)}, u32[]{:S(2)}) %all-to-all-start.2) | async-done | bytes 1048608 | tf_op jit(solution)/shard_map/all_to_all | solution.py:127
  189.2 6.0 %all-to-all-start.6 = ((bf16[16,64,128]{2,1,0:T(8,128)(2,1)}), bf16[16,64,128]{2,1,0:T(8,128)(2,1)}, u32[]{:S(2)}, u32[]{:S(2)}) async-start(bf16[16,64,128]{2,1,0:T(8,128)(2,1)} %multiply_reduce_fusion), calls=%async_computation.7 | async-start | bytes 524288 | tf_op jit(solution)/shard_map/all_to_all | solution.py:84
  195.3 1.9 fusion.13
  197.2 1.7 copy.144
  198.8 2.0 bitcast_bitcast_fusion
  200.9 2.8 %all-to-all-done.6 = bf16[16,64,128]{2,1,0:T(8,128)(2,1)} async-done(((bf16[16,64,128]{2,1,0:T(8,128)(2,1)}), bf16[16,64,128]{2,1,0:T(8,128)(2,1)}, u32[]{:S(2)}, u32[]{:S(2)}) %all-to-all-start.6) | async-done | bytes 262176 | tf_op jit(solution)/shard_map/all_to_all | solution.py:84
  203.8 4.2 %all-to-all-start.3 = ((bf16[16,128,128]{2,1,0:T(8,128)(2,1)}), bf16[16,128,128]{2,1,0:T(8,128)(2,1)}, u32[]{:S(2)}, u32[]{:S(2)}) async-start(bf16[16,128,128]{2,1,0:T(8,128)(2,1)} %bitcast_bitcast_fusion), calls=%async_computation.4 | async-start | bytes 1048576 | tf_op jit(solution)/shard_map/all_to_all | solution.py:212
  208.1 1.3 convolution_bitcast_fusion.3
  209.4 1.8 fusion.12
  211.2 1.7 copy.143
  212.9 1.2 fusion.59
  215.1 1.8 copy.142
  217.0 4.0 %all-to-all-done.3 = bf16[16,128,128]{2,1,0:T(8,128)(2,1)} async-done(((bf16[16,128,128]{2,1,0:T(8,128)(2,1)}), bf16[16,128,128]{2,1,0:T(8,128)(2,1)}, u32[]{:S(2)}, u32[]{:S(2)}) %all-to-all-start.3) | async-done | bytes 524320 | tf_op jit(solution)/shard_map/all_to_all | solution.py:212
  221.6 3.8 %all-to-all-start.7 = ((f32[16,1,16]{2,1,0:T(1,128)}), f32[16,1,16]{2,1,0:T(1,128)S(1)}, u32[]{:S(2)}, u32[]{:S(2)}) async-start(f32[16,1,16]{2,1,0:T(1,128)} %broadcast_in_dim.100), calls=%async_computation.8 | async-start | bytes 16384 | tf_op jit(solution)/shard_map/all_to_all | solution.py:53
  225.5 3.9 %fusion.85 = f32[128,1024]{1,0:T(8,128)} fusion(bf16[2048,128]{1,0:T(8,128)(2,1)} %bitcast.29, bf16[2048,1024]{1,0:T(8,128)(2,1)} %all-gather.8.cloned.1.call-done), kind=kOutput, calls=%fused_computation.144 | convolution fusion | flops 536870912 | bytes 5242880 | tf_op jit(solution)/shard_map/td,ti->di/dot_general | solution.py:219
  229.5 3.2 %all-to-all-done.7 = f32[16,1,16]{2,1,0:T(1,128)S(1)} async-done(((f32[16,1,16]{2,1,0:T(1,128)}), f32[16,1,16]{2,1,0:T(1,128)S(1)}, u32[]{:S(2)}, u32[]{:S(2)}) %all-to-all-start.7) | async-done | bytes 1056 | tf_op jit(solution)/shard_map/all_to_all | solution.py:53
  233.6 4.4 %fusion.1 = bf16[1,2048,512]{2,1,0:T(8,128)(2,1)} fusion(bf16[512,2048]{1,0:T(8,128)(2,1)} %all-gather.6.cloned.1.call-done, bf16[512,512]{1,0:T(8,128)(2,1)S(1)} %copy-done.21), kind=kOutput, calls=%fused_computation.6 | convolution fusion | flops 1074790400 | bytes 4718592 | tf_op jit(solution)/shard_map/rd,rf->df/dot_general | solution.py:209
  238.0 2.9 %fusion = bf16[1,2048,512]{2,1,0:T(8,128)(2,1)} fusion(bf16[512,2048]{1,0:T(8,128)(2,1)S(1)} %copy-done.39, bf16[1,512,512]{2,1,0:T(8,128)(2,1)S(1)} %copy-done.41, f32[512,512]{1,0:T(8,128)S(1)} %copy-done.45, bf16[1,512,512]{2,1,0:T(8,128)(2,1)S(1)} %copy-done.43), kind=kOutput, calls=%fused_computation.5 | convolution fusion | flops 1079508992 | bytes 6291456 | tf_op jit(solution)/shard_map/rd,rf->df/dot_general | solution.py:206
  (152 shorter events, 18.4 us)
Async XLA Ops:
  8.0 52.1 %copy-start = (bf16[1,2048,512]{2,1,0:T(8,128)(2,1)S(1)}, bf16[1,2048,512]{2,1,0:T(8,128)(2,1)}, u32[]{:S(2)}) copy-start(bf16[1,2048,512]{2,1,0:T(8,128)(2,1)} %param.23) | copy-start | bytes 6291460
  8.0 48.2 %all-gather.4.cloned.1.call-start = ((), (), s32[]{:S(2)}) async-start(), calls=%async_computation.9 | async-start | bytes 3145728 | tf_op jit(solution)/shard_map/all_gather | solution.py:134
  10.3 36.9 %copy-start.31 = (s32[2,128]{1,0:T(2,128)}, s32[2,128]{1,0:T(2,128)S(1)}, u32[]{:S(2)}) copy-start(s32[2,128]{1,0:T(2,128)S(1)} %add_bitcast_fusion) | copy-start | bytes 3076
  11.3 45.0 %copy-start.40 = (bf16[1,512,512]{2,1,0:T(8,128)(2,1)S(1)}, bf16[1,512,512]{2,1,0:T(8,128)(2,1)}, u32[]{:S(2)}) copy-start(bf16[1,512,512]{2,1,0:T(8,128)(2,1)} %param.21) | copy-start | bytes 1572868
  11.3 45.0 %copy-start.42 = (bf16[1,512,512]{2,1,0:T(8,128)(2,1)S(1)}, bf16[1,512,512]{2,1,0:T(8,128)(2,1)}, u32[]{:S(2)}) copy-start(bf16[1,512,512]{2,1,0:T(8,128)(2,1)} %param.22) | copy-start | bytes 1572868
  47.2 28.7 %reduce-scatter.2.cloned.1.call-start = ((), (), s32[]{:S(2)}) async-start(), calls=%async_computation.10 | async-start | bytes 3145728 | tf_op jit(solution)/shard_map/reduce_scatter | solution.py:147
  60.1 1.8 copy-start.44
  60.1 1.8 copy-start.20
  60.1 2.1 copy-start.11
  64.9 1.5 copy-start.23
  64.9 1.7 copy-start.35
  64.9 160.6 %all-gather.8.cloned.1.call-start = ((), (), s32[]{:S(2)}) async-start(), calls=%async_computation.12 | async-start | bytes 4456448 | tf_op jit(solution)/shard_map/all_gather | solution.py:188
  66.0 2.6 %copy-start.9 = (bf16[1,16,64,128]{3,2,1,0:T(8,128)(2,1)}, bf16[1,16,64,128]{3,2,1,0:T(8,128)(2,1)S(1)}, u32[]{:S(2)}) copy-start(bf16[1,16,64,128]{3,2,1,0:T(8,128)(2,1)S(1)} %convert_element_type.154) | copy-start | bytes 786436
  66.2 2.4 copy-start.15
  66.2 2.4 copy-start.13
  66.4 2.1 copy-start.16
  66.6 1.9 copy-start.27
  72.4 1.9 copy-start.33
  75.5 7.4 %copy-start.34 = (bf16[1024]{0:T(1024)(128)(2,1)S(1)}, bf16[1024]{0:T(1024)(128)(2,1)}, u32[]{:S(2)}) copy-start(bf16[1024]{0:T(1024)(128)(2,1)} %param.27) | copy-start | bytes 6148
  75.5 8.0 %copy-start.32 = (s32[2,128]{1,0:T(2,128)S(1)}, s32[2,128]{1,0:T(2,128)}, u32[]{:S(2)}) copy-start(s32[2,128]{1,0:T(2,128)} %copy-done.31) | copy-start | bytes 3076
  75.5 37.6 %copy-start.37 = (f32[16]{0:T(128)S(1)}, f32[16]{0:T(128)}, u32[]{:S(2)}) copy-start(f32[16]{0:T(128)} %copy-done.36) | copy-start | bytes 196
  75.9 37.2 %all-to-all-start.1 = ((bf16[16,32,1024]{2,1,0:T(8,128)(2,1)}), bf16[16,32,1024]{2,1,0:T(8,128)(2,1)}, u32[]{:S(2)}, u32[]{:S(2)}) async-start(bf16[16,32,1024]{2,1,0:T(8,128)(2,1)} %bitcast.217), calls=%async_computation.2 | async-start | bytes 2097152 | tf_op jit(solution)/shard_map/all_to_all | solution.py:150
  83.5 40.2 %copy-start.18 = (bf16[512,128]{1,0:T(8,128)(2,1)}, bf16[512,128]{1,0:T(8,128)(2,1)S(1)}, u32[]{:S(2)}) copy-start(bf16[512,128]{1,0:T(8,128)(2,1)S(1)} %fusion.52) | copy-start | bytes 393220
  113.7 23.7 %all-to-all-start.4 = ((f32[16,1,16]{2,1,0:T(1,128)}), f32[16,1,16]{2,1,0:T(1,128)}, u32[]{:S(2)}, u32[]{:S(2)}) async-start(f32[16,1,16]{2,1,0:T(1,128)} %broadcast_in_dim.61), calls=%async_computation.5 | async-start | bytes 16384 | tf_op jit(solution)/shard_map/all_to_all | solution.py:53
  129.0 4.2 %copy-start.5 = (f32[16,8,4,256]{3,1,2,0:T(8,128)S(1)}, f32[16,8,4,256]{3,1,2,0:T(8,128)}, u32[]{:S(2)}) copy-start(f32[16,8,4,256]{3,1,2,0:T(8,128)} %copy-done.4) | copy-start | bytes 1572868
  131.1 2.1 copy-start.6
  131.1 2.1 copy-start.7
  131.2 2.1 copy-start.8
  131.2 2.1 copy-start.12
  131.2 2.1 copy-start.30
  137.4 21.5 %all-to-all-start.5 = ((bf16[16,64,128]{2,1,0:T(8,128)(2,1)}), bf16[16,64,128]{2,1,0:T(8,128)(2,1)}, u32[]{:S(2)}, u32[]{:S(2)}) async-start(bf16[16,64,128]{2,1,0:T(8,128)(2,1)} %bitcast.216), calls=%async_computation.6 | async-start | bytes 524288 | tf_op jit(solution)/shard_map/all_to_all | solution.py:76
  158.9 30.3 %all-to-all-start.2 = ((bf16[16,32,1024]{2,1,0:T(8,128)(2,1)}), bf16[16,32,1024]{2,1,0:T(8,128)(2,1)}, u32[]{:S(2)}, u32[]{:S(2)}) async-start(bf16[16,32,1024]{2,1,0:T(8,128)(2,1)} %bitcast.202), calls=%async_computation.3 | async-start | bytes 2097152 | tf_op jit(solution)/shard_map/all_to_all | solution.py:127
  166.6 5.9 %copy-start.10 = (bf16[1,16,64,128]{3,2,1,0:T(8,128)(2,1)S(1)}, bf16[1,16,64,128]{3,2,1,0:T(8,128)(2,1)}, u32[]{:S(2)}) copy-start(bf16[1,16,64,128]{3,2,1,0:T(8,128)(2,1)} %copy-done.9) | copy-start | bytes 786436
  166.6 6.9 %copy-start.28 = (pred[128,128]{1,0:T(8,128)(4,1)S(1)}, pred[128,128]{1,0:T(8,128)(4,1)}, u32[]{:S(2)}) copy-start(pred[128,128]{1,0:T(8,128)(4,1)} %copy-done.27) | copy-start | bytes 49156
  173.6 21.7 %copy-start.17 = (bf16[128,4,128]{0,2,1:T(8,128)(2,1)S(1)}, bf16[128,4,128]{0,2,1:T(8,128)(2,1)}, u32[]{:S(2)}) copy-start(bf16[128,4,128]{0,2,1:T(8,128)(2,1)} %copy-done.16) | copy-start | bytes 393220
  189.2 14.6 %all-to-all-start.6 = ((bf16[16,64,128]{2,1,0:T(8,128)(2,1)}), bf16[16,64,128]{2,1,0:T(8,128)(2,1)}, u32[]{:S(2)}, u32[]{:S(2)}) async-start(bf16[16,64,128]{2,1,0:T(8,128)(2,1)} %multiply_reduce_fusion), calls=%async_computation.7 | async-start | bytes 524288 | tf_op jit(solution)/shard_map/all_to_all | solution.py:84
  195.2 38.3 %all-gather.6.cloned.1.call-start = ((), (), s32[]{:S(2)}) async-start(), calls=%async_computation.11 | async-start | bytes 3145728 | tf_op jit(solution)/shard_map/all_gather | solution.py:134
  198.8 9.2 %copy-start.26 = (f32[128,16]{0,1:T(8,128)S(1)}, f32[128,16]{0,1:T(8,128)}, u32[]{:S(2)}) copy-start(f32[128,16]{0,1:T(8,128)} %get-tuple-element.77) | copy-start | bytes 24580
  200.9 12.0 %copy-start.14 = (bf16[128,4,128]{2,1,0:T(4,128)(2,1)S(1)}, bf16[128,4,128]{2,1,0:T(4,128)(2,1)}, u32[]{:S(2)}) copy-start(bf16[128,4,128]{2,1,0:T(4,128)(2,1)} %copy-done.13) | copy-start | bytes 393220
  203.8 17.2 %all-to-all-start.3 = ((bf16[16,128,128]{2,1,0:T(8,128)(2,1)}), bf16[16,128,128]{2,1,0:T(8,128)(2,1)}, u32[]{:S(2)}, u32[]{:S(2)}) async-start(bf16[16,128,128]{2,1,0:T(8,128)(2,1)} %bitcast_bitcast_fusion), calls=%async_computation.4 | async-start | bytes 1048576 | tf_op jit(solution)/shard_map/all_to_all | solution.py:212
  208.0 6.1 %copy-start.3 = (bf16[16,128,128]{2,1,0:T(8,128)(2,1)S(1)}, bf16[16,128,128]{2,1,0:T(8,128)(2,1)}, u32[]{:S(2)}) copy-start(bf16[16,128,128]{2,1,0:T(8,128)(2,1)} %copy-done.2) | copy-start | bytes 1572868
  221.6 11.1 %all-to-all-start.7 = ((f32[16,1,16]{2,1,0:T(1,128)}), f32[16,1,16]{2,1,0:T(1,128)S(1)}, u32[]{:S(2)}, u32[]{:S(2)}) async-start(f32[16,1,16]{2,1,0:T(1,128)} %broadcast_in_dim.100), calls=%async_computation.8 | async-start | bytes 16384 | tf_op jit(solution)/shard_map/all_to_all | solution.py:53
  225.5 7.2 %copy-start.38 = (pred[16]{0:T(512)(128)(4,1)S(1)}, pred[16]{0:T(512)(128)(4,1)}, u32[]{:S(2)}) copy-start(pred[16]{0:T(512)(128)(4,1)} %iota_compare_fusion.11) | copy-start | bytes 52
  225.5 8.0 %copy-start.21 = (bf16[512,512]{1,0:T(8,128)(2,1)S(1)}, bf16[512,512]{1,0:T(8,128)(2,1)}, u32[]{:S(2)}) copy-start(bf16[512,512]{1,0:T(8,128)(2,1)} %copy-done.20) | copy-start | bytes 1572868
  233.6 4.4 %copy-start.41 = (bf16[1,512,512]{2,1,0:T(8,128)(2,1)S(1)}, bf16[1,512,512]{2,1,0:T(8,128)(2,1)}, u32[]{:S(2)}) copy-start(bf16[1,512,512]{2,1,0:T(8,128)(2,1)} %param.21) | copy-start | bytes 1572868
  233.6 4.4 %copy-start.39 = (bf16[512,2048]{1,0:T(8,128)(2,1)S(1)}, bf16[512,2048]{1,0:T(8,128)(2,1)}, u32[]{:S(2)}) copy-start(bf16[512,2048]{1,0:T(8,128)(2,1)} %all-gather.6.cloned.1.call-done) | copy-start | bytes 6291460
  233.6 4.4 %copy-start.43 = (bf16[1,512,512]{2,1,0:T(8,128)(2,1)S(1)}, bf16[1,512,512]{2,1,0:T(8,128)(2,1)}, u32[]{:S(2)}) copy-start(bf16[1,512,512]{2,1,0:T(8,128)(2,1)} %param.22) | copy-start | bytes 1572868
  233.6 4.4 %copy-start.45 = (f32[512,512]{1,0:T(8,128)S(1)}, f32[512,512]{1,0:T(8,128)}, u32[]{:S(2)}) copy-start(f32[512,512]{1,0:T(8,128)} %copy-done.44) | copy-start | bytes 3145732
  (9 other events, 9.1 us)
Sparse Core Ops, SparseCore 0:
  47.3 8.8 all-gather.3
  65.0 10.7 reduce-scatter.1
Sparse Core Ops, SparseCore 1:
  75.6 89.1 all-gather.7
  200.9 11.7 all-gather.5
where the time goes:
time: 250 us; the launch traced here: 248 us
  waiting for transfers between devices  69.7 us (28%)
  matrix products  47.4 us (19%)
  starting transfers between devices  41.5 us (17%)
  blocking collectives  36.7 us (15%)
  local copies, waits for them, and re-layouts  21.3 us (9%)
  between operations  16.3 us (7%)
  other arithmetic  15.4 us (6%)
    all_to_all x1, blocking collectives, dispatch(): lax.all_to_all(rows.astype(jnp.bfloat16).reshape(expert_count, capacity,...  34.6 us
    all_to_all x1, waiting for transfers between devices, body(): lax.all_to_all(summed.reshape(expert_count, capacity, -1), 'sp', split_ax...  27.8 us
    all_to_all x1, waiting for transfers between devices, later_states(): lax.all_to_all(block_state.astype(jnp.bfloat16).reshape(count, rows, widt...  12.2 us
    all_to_all x1, waiting for transfers between devices, dispatch(): lax.all_to_all(rows.astype(jnp.bfloat16).reshape(expert_count, capacity,...  10.2 us
    all_to_all x2, starting transfers between devices, exchange(): return lax.all_to_all(pieces, 'sp', split_axis=0, concat_axis=0, tiled=True)  10.1 us
    unnamed x99, local copies, waits for them, and re-layouts  9.1 us
    all_gather x2, waiting for transfers between devices, dispatch(): return lax.all_gather(arrived, 'tp', axis=1, tiled=True)  9.01 us
    all_to_all x1, starting transfers between devices, dispatch(): lax.all_to_all(rows.astype(jnp.bfloat16).reshape(expert_count, capacity,...  7.18 us
  transfers between devices with their start and end apart: 11, of which 8 were waited for; matrix products, arithmetic and copies ran while one was open for 25% of the time, Pallas kernels for 0%

commit v1 on v0

--- a/solution.py
+++ b/solution.py
@@ -1,8 +1,13 @@
+import functools
+
 import jax
 import jax.numpy as jnp
 from jax import lax
 from jax.sharding import PartitionSpec as P
 
+from jax.experimental import pallas as pl
+from jax.experimental.pallas import tpu as pltpu
+
 HEAD_DIM = 64
 STATE = 128
 
@@ -10,6 +15,584 @@
 rms_epsilon = 1e-05
 clamp_limit = 7.0
 swish_alpha = 1.702
+
+
+MESH = pl.DeviceIdType.MESH
+f32, bf16 = jnp.float32, jnp.bfloat16
+
+
+def dot_nn(a, b):
+    return jnp.dot(a, b, preferred_element_type=f32)
+
+
+def dot_nt(a, b):
+    return lax.dot_general(a, b, (((1,), (1,)), ((), ())), preferred_element_type=f32)
+
+
+def dot_tn(a, b):
+    return lax.dot_general(a, b, (((0,), (0,)), ((), ())), preferred_element_type=f32)
+
+
+def dot_full(a, b):
+    return jnp.dot(a, b, precision=lax.Precision.HIGHEST, preferred_element_type=f32)
+
+
+def xor(value, bits):
+    bit = 1
+    while bit <= bits:
+        if bits & bit:
+            value = value + bit * (1 - 2 * ((value // bit) % 2))
+        bit *= 2
+    return value
+
+
+def iota(shape, dim):
+    return lax.broadcasted_iota(jnp.int32, shape, dim)
+
+
+def aligned(value, unit):
+    return pl.multiple_of(value, unit)
+
+
+def fused(
+    dims,
+    choice, choice_t, weight_t, decay, decay_t, gain, scan_x, gate_x, b_in, c_in, entry,
+    cot_hbm, hid_hbm, gpre_hbm, upre_hbm, wg_hbm, wu_hbm, wd_hbm, wo_hbm,
+    owg, owu, owd, oproj, oscan, ogate, ob, oc, odecay,
+    cot, hid, gpre, upre, wg, wu, wd, wo,
+    send_g, send_h, g_full, h_full, part_send, part_recv, ret_send, ret_recv,
+    active, gate_grad, up_grad, places_t,
+    mixed_z, hidden, hidden_z, rs_send, rs_recv,
+    scan_out, unit, inv_rms, gy, mix_t, decays, growth_s, tail_s, entry_b, block_state,
+    st_send, st_recv, rv_send, rv_recv, tot_send, tot_recv, gat_send, gat_recv,
+    grad_wg, grad_wu, grad_wd,
+    in_sem, out_sem, g_s, g_r, h_s, h_r, ret_s, ret_r, st_s, st_r, rv_s, rv_r,
+    tot_s, tot_r, gat_s, gat_r, fg_s, fg_r, fh_s, fh_r, px_s, px_r, mz_s, mz_r,
+    gh_s, gh_r, hz_s, hz_r, fz_s, fz_r, rs_s, rs_r,
+):
+    n, outer, cap = dims
+    inner = n // outer
+    tokens, half = cot.shape
+    rows = n * cap
+    zrows = inner * cap
+    heads = decay.shape[1]
+    groups = b_in.shape[1] // STATE
+    pairs_in_group = heads // groups // 2
+    gwidth = pairs_in_group * 128
+    per_half = outer // 2
+    dchunk = hidden.shape[2]
+    srows = st_send.shape[0] // n
+    dcols = dchunk // inner
+    thalf = tokens // 2
+    me = lax.axis_index("sp")
+    tp = lax.axis_index("tp")
+    other = 1 - tp
+    my_z = me // inner
+    my_q = me % inner
+    peers = [xor(me, k) for k in range(n)]
+
+    def remote(src, dst, s, r, sp_id, tp_id):
+        return pltpu.make_async_remote_copy(
+            src_ref=src, dst_ref=dst, send_sem=s, recv_sem=r,
+            device_id=(sp_id, tp_id), device_id_type=MESH,
+        )
+
+    def rowblock(block, size):
+        return pl.ds(aligned(block * size, size), size)
+
+    barrier = pltpu.get_barrier_semaphore()
+    for k in range(1, n):
+        pl.semaphore_signal(barrier, inc=1, device_id=(peers[k], tp), device_id_type=MESH)
+    pl.semaphore_signal(barrier, inc=1, device_id=(me, other), device_id_type=MESH)
+
+    own_cols = pl.ds(aligned(tp * half, half), half)
+    loads = [
+        pltpu.make_async_copy(cot_hbm.at[:, own_cols], cot, in_sem.at[0]),
+        pltpu.make_async_copy(hid_hbm.at[:, own_cols], hid, in_sem.at[1]),
+        pltpu.make_async_copy(wd_hbm, wd, in_sem.at[2]),
+        pltpu.make_async_copy(gpre_hbm, gpre, in_sem.at[3]),
+        pltpu.make_async_copy(upre_hbm, upre, in_sem.at[4]),
+        pltpu.make_async_copy(wg_hbm, wg, in_sem.at[5]),
+        pltpu.make_async_copy(wu_hbm, wu, in_sem.at[6]),
+        pltpu.make_async_copy(wo_hbm, wo, in_sem.at[7]),
+    ]
+    for load in loads:
+        load.start()
+
+    expert_s = iota((n, tokens), 0)
+    first_t = choice_t[0:1, :] == expert_s
+    second_t = choice_t[1:2, :] == expert_s
+    row_id = iota((tokens, tokens), 0)
+    col_id = iota((tokens, tokens), 1)
+    named_t = jnp.where(first_t | second_t, 1.0, 0.0).astype(bf16)
+    before_t = jnp.where(row_id < col_id, 1.0, 0.0).astype(bf16)
+    base_t = dot_nn(named_t, before_t) + (cap * expert_s).astype(f32)
+    slot0_t = jnp.sum(jnp.where(first_t, base_t, 0.0), axis=0, keepdims=True)
+    slot1_t = jnp.sum(jnp.where(second_t, base_t, 0.0), axis=0, keepdims=True)
+
+    expert_l = iota((tokens, n), 1)
+    first = choice[:, 0:1] == expert_l
+    second = choice[:, 1:2] == expert_l
+    named = jnp.where(first | second, 1.0, 0.0).astype(bf16)
+    before = jnp.where(row_id > col_id, 1.0, 0.0).astype(bf16)
+    base = dot_nn(before, named) + (cap * expert_l).astype(f32)
+    slot0 = jnp.sum(jnp.where(first, base, 0.0), axis=1, keepdims=True)
+    slot1 = jnp.sum(jnp.where(second, base, 0.0), axis=1, keepdims=True)
+    slot_l = iota((tokens, rows), 1).astype(f32)
+    places_t[...] = jnp.where((slot_l == slot0) | (slot_l == slot1), 1.0, 0.0).astype(bf16)
+
+    loads[0].wait()
+    loads[1].wait()
+    for z in range(outer):
+        part = slice(z * zrows, (z + 1) * zrows)
+        slot_s = (iota((zrows, tokens), 0) + z * zrows).astype(f32)
+        in_first = slot_s == slot0_t
+        in_second = slot_s == slot1_t
+        places = jnp.where(in_first | in_second, 1.0, 0.0).astype(bf16)
+        scale = jnp.sum(
+            jnp.where(in_first, weight_t[0:1, :], 0.0) + jnp.where(in_second, weight_t[1:2, :], 0.0),
+            axis=1, keepdims=True,
+        )
+        send_g[part, :] = (dot_nn(places, cot[...]) * scale).astype(bf16)
+        send_h[part, :] = dot_nn(places, hid[...]).astype(bf16)
+
+    pl.semaphore_wait(barrier, n)
+
+    def all_to_all(send, recv, size, s, r):
+        mine = rowblock(me, size)
+        return [None] + [
+            remote(send.at[rowblock(peers[k], size)], recv.at[mine], s.at[k], r.at[k], peers[k], tp)
+            for k in range(1, n)
+        ]
+
+    own_rows = rowblock(me, cap)
+    copy_g = all_to_all(send_g, g_full.at[tp], cap, g_s, g_r)
+    copy_h = all_to_all(send_h, h_full.at[tp], cap, h_s, h_r)
+    copy_ret = all_to_all(ret_send, ret_recv, cap, ret_s, ret_r)
+    copy_st = all_to_all(st_send, st_recv, srows, st_s, st_r)
+    copy_rv = all_to_all(rv_send, rv_recv, srows, rv_s, rv_r)
+    far_first = list(range(n - 1, 0, -1))
+    for k in far_first:
+        copy_g[k].start()
+    g_full[tp, own_rows, :] = send_g[own_rows, :]
+    h_full[tp, own_rows, :] = send_h[own_rows, :]
+
+    causal = row_id >= col_id
+    causal_f = jnp.where(causal, 1.0, 0.0)
+    anti_f = jnp.where(row_id <= col_id, 1.0, 0.0)
+    cum = dot_full(causal_f, decay[...])
+    cum_t = dot_full(decay_t[...], anti_f)
+    growth_s[...] = jnp.exp(cum)
+    tail_s[...] = jnp.exp(cum[tokens - 1:tokens, :] - cum)
+    tot_send[...] = jnp.zeros(tot_send.shape, f32)
+    tot_send[0:1, 0:heads] = cum[tokens - 1:tokens, :]
+    tot_recv[me] = tot_send[...]
+    copy_tot = [None] + [
+        remote(tot_send, tot_recv.at[me], tot_s.at[k], tot_r.at[k], peers[k], tp)
+        for k in range(1, n)
+    ]
+    for k in far_first:
+        copy_tot[k].start()
+    lane = iota((1, 128), 1)
+    low_lane = lane < HEAD_DIM
+    low = jnp.where(low_lane, 1.0, 0.0)
+    low_b, high_b = low.astype(bf16), (1.0 - low).astype(bf16)
+
+    def spread(columns, pair):
+        return jnp.where(
+            low_lane, columns[:, 2 * pair:2 * pair + 1], columns[:, 2 * pair + 1:2 * pair + 2]
+        )
+
+    def tile(index):
+        return slice(index * 128, (index + 1) * 128)
+
+    def group_cols(g):
+        return slice(g * gwidth, (g + 1) * gwidth)
+
+    entry_b[...] = entry[...].astype(bf16)
+    for g in range(groups):
+        b_g, c_g = b_in[:, tile(g)], c_in[:, tile(g)]
+        inner_prod = dot_nt(c_g, b_g)
+        inner_t = dot_nt(b_g, c_g)
+        squares = jnp.zeros((tokens, 1), f32)
+        gated = []
+        for pair in range(g * pairs_in_group, (g + 1) * pairs_in_group):
+            mats = []
+            for h in (2 * pair, 2 * pair + 1):
+                gap = cum[:, h:h + 1] - cum_t[h:h + 1, :]
+                fade = jnp.exp(jnp.where(causal, gap, -jnp.inf))
+                decays[h] = fade
+                mats.append((inner_prod * fade).astype(bf16))
+                gap_t = cum_t[h:h + 1, :] - cum[:, h:h + 1]
+                mix_t[pair, :, tile(h % 2)] = (
+                    inner_t * jnp.exp(jnp.where(row_id <= col_id, gap_t, -jnp.inf))
+                ).astype(bf16)
+            x = scan_x[:, tile(pair)]
+            y = dot_nn(mats[0], x * low_b) + dot_nn(mats[1], x * high_b)
+            carry = dot_nt(c_g, entry_b[tile(pair), :])
+            out = y + carry * spread(growth_s, pair)
+            scan_out[:, tile(pair)] = out
+            gate = gate_x[:, tile(pair)].astype(f32)
+            value = out * (gate * jax.nn.sigmoid(gate))
+            squares = squares + jnp.sum(value * value, axis=1, keepdims=True)
+            gated.append(value)
+        inv = lax.rsqrt(squares * (1.0 / gwidth) + rms_epsilon)
+        inv_rms[g] = inv
+        for i, value in enumerate(gated):
+            cols = tile(g * pairs_in_group + i)
+            flat = value * inv
+            unit[:, cols] = flat
+            mixed_z[my_z, :, cols] = (flat * gain[:, cols].astype(f32)).astype(bf16)
+
+    copy_mz = [None] + [
+        remote(
+            mixed_z.at[my_z], mixed_z.at[my_z], mz_s.at[j], mz_r.at[j],
+            xor(my_z, j) * inner + my_q, tp,
+        )
+        for j in range(1, outer)
+    ]
+
+    for i in range(2, 7):
+        loads[i].wait()
+    fwd_g, fwd_h, px = [], [], []
+    for j in range(outer):
+        zpart = rowblock(xor(my_z, j), zrows)
+        fwd_g.append(
+            remote(g_full.at[tp, zpart], g_full.at[tp, zpart], fg_s.at[j], fg_r.at[j], me, other)
+        )
+        fwd_h.append(
+            remote(h_full.at[tp, zpart], h_full.at[tp, zpart], fh_s.at[j], fh_r.at[j], me, other)
+        )
+        px.append(remote(part_send.at[j], part_recv.at[j], px_s.at[j], px_r.at[j], me, other))
+    for j in range(outer):
+        for k in range(j * inner, (j + 1) * inner):
+            if k:
+                copy_g[k].wait_recv()
+        fwd_g[j].start()
+        fwd_g[j].wait_recv()
+        zpart = rowblock(xor(my_z, j), zrows)
+        act = dot_nt(g_full[0, zpart, :], wd[:, 0:half])
+        act = act + dot_nt(g_full[1, zpart, :], wd[:, half:2 * half])
+        gate_full = gpre[zpart, :].astype(f32)
+        up_full = upre[zpart, :].astype(f32)
+        gate_clip = jnp.minimum(gate_full, clamp_limit)
+        up_clip = jnp.clip(up_full, -clamp_limit, clamp_limit)
+        sig = jax.nn.sigmoid(swish_alpha * gate_clip)
+        swish = gate_clip * sig
+        active[zpart, :] = ((up_clip + 1.0) * swish).astype(bf16)
+        inside = (up_full > -clamp_limit) & (up_full < clamp_limit)
+        ug = jnp.where(inside, act * swish, 0.0).astype(bf16)
+        slope = sig + swish_alpha * gate_clip * sig * (1.0 - sig)
+        gg = jnp.where(gate_full < clamp_limit, act * (up_clip + 1.0) * slope, 0.0).astype(bf16)
+        up_grad[zpart, :] = ug
+        gate_grad[zpart, :] = gg
+        part_send[j] = (dot_nt(gg, wg[other]) + dot_nt(ug, wu[other])).astype(bf16)
+        px[j].start()
+        own = (dot_nt(gg, wg[tp]) + dot_nt(ug, wu[tp])).astype(bf16)
+        px[j].wait_recv()
+        ret_send[zpart, :] = (own.astype(f32) + part_recv[j].astype(f32)).astype(bf16)
+        if j == 0:
+            ret_recv[own_rows, :] = ret_send[own_rows, :]
+        for k in range(j * inner, (j + 1) * inner):
+            if k:
+                copy_ret[k].start()
+
+    for k in far_first:
+        copy_h[k].start()
+
+    def down_step(i, carry):
+        cols = pl.ds(aligned(i * 256, 256), 256)
+        for s in range(2):
+            grad_wd[s, :, cols] = dot_tn(active[...], g_full[s, :, cols]).astype(bf16)
+        return carry
+
+    lax.fori_loop(0, half // 256, down_step, 0)
+    stores = [
+        pltpu.make_async_copy(grad_wd.at[0], owd.at[:, 0:half], out_sem.at[0]),
+        pltpu.make_async_copy(grad_wd.at[1], owd.at[:, half:2 * half], out_sem.at[1]),
+    ]
+    stores[0].start()
+    stores[1].start()
+
+    for k in range(1, n):
+        copy_ret[k].wait_recv()
+    moe = dot_nn(places_t[...], ret_recv[...])
+    for i in range(per_half):
+        cols = slice(i * dchunk, (i + 1) * dchunk)
+        hidden[tp * per_half + i] = (cot[:, cols].astype(f32) + moe[:, cols]).astype(bf16)
+    own_chunks = pl.ds(tp * per_half, per_half)
+    copy_gh = remote(hidden.at[own_chunks], hidden.at[own_chunks], gh_s, gh_r, me, other)
+    copy_gh.start()
+    loads[7].wait()
+    copy_gh.wait_recv()
+    hidden_z[my_z] = hidden[my_z]
+    my_tokens = pl.ds(aligned(tp * thalf, thalf), thalf)
+    copy_hz, fwd_z = [None], [None]
+    for j in range(1, outer):
+        z = xor(my_z, j)
+        copy_hz.append(
+            remote(
+                hidden.at[z, my_tokens], hidden_z.at[my_z, my_tokens],
+                hz_s.at[j], hz_r.at[j], z * inner + my_q, tp,
+            )
+        )
+        fwd_z.append(
+            remote(
+                hidden_z.at[z, my_tokens], hidden_z.at[z, my_tokens],
+                fz_s.at[j], fz_r.at[j], me, other,
+            )
+        )
+    for j in range(outer - 1, 0, -1):
+        copy_hz[j].start()
+
+    for g in range(groups):
+        c_g = c_in[:, tile(g)]
+        gcols = group_cols(g)
+        gm = dot_nt(hidden[0], wo[gcols, 0:dchunk])
+        for i in range(1, outer):
+            gm = gm + dot_nt(hidden[i], wo[gcols, i * dchunk:(i + 1) * dchunk])
+        gu = gm * gain[:, gcols].astype(f32)
+        flat = unit[:, gcols]
+        mean = jnp.sum(gu * flat, axis=1, keepdims=True) * (1.0 / gwidth)
+        gg = inv_rms[g] * (gu - flat * mean)
+        gate = gate_x[:, gcols].astype(f32)
+        sig = jax.nn.sigmoid(gate)
+        ogate[:, gcols] = (
+            gg * scan_out[:, gcols] * sig * (1.0 + gate * (1.0 - sig))
+        ).astype(bf16)
+        grad_y = gg * (gate * sig)
+        gy[:, gcols] = grad_y
+        for i in range(pairs_in_group):
+            pair = g * pairs_in_group + i
+            grown = (grad_y[:, tile(i)] * spread(growth_s, pair)).astype(bf16)
+            st_send[tile(pair), :] = dot_tn(grown, c_g).astype(bf16)
+    own_st = rowblock(me, srows)
+    for k in far_first:
+        copy_st[k].start()
+    st_recv[own_st, :] = st_send[own_st, :]
+    for j in range(outer - 1, 0, -1):
+        copy_mz[j].start()
+
+    for g in range(groups):
+        b_g, c_g = b_in[:, tile(g)], c_in[:, tile(g)]
+        gw = jnp.zeros((tokens, tokens), f32)
+        gc = jnp.zeros((tokens, STATE), f32)
+        for i in range(pairs_in_group):
+            pair = g * pairs_in_group + i
+            gy_t = gy[:, tile(pair)]
+            gyb = gy_t.astype(bf16)
+            x = scan_x[:, tile(pair)]
+            gw = gw + dot_nt(gyb * low_b, x) * decays[2 * pair]
+            gw = gw + dot_nt(gyb * high_b, x) * decays[2 * pair + 1]
+            grown = (gy_t * spread(growth_s, pair)).astype(bf16)
+            gc = gc + dot_nn(grown, entry_b[tile(pair), :])
+        gwb = gw.astype(bf16)
+        oc[:, tile(g)] = (gc + dot_nn(gwb, b_g)).astype(bf16)
+        block_state[g] = dot_tn(gwb, c_g)
+
+    for k in range(1, n):
+        copy_tot[k].wait_recv()
+        copy_st[k].wait_recv()
+    my_head = (me * srows) // HEAD_DIM
+    rev = jnp.zeros((srows, STATE), f32)
+    for b in range(n - 1, -1, -1):
+        part = slice(b * srows, (b + 1) * srows)
+        rv_send[part, :] = rev.astype(bf16)
+        if b:
+            total = jnp.sum(
+                jnp.where(lane == my_head, tot_recv[b, 0:1, :], 0.0), axis=1, keepdims=True
+            )
+            rev = st_recv[part, :].astype(f32) + jnp.exp(total) * rev
+    for k in far_first:
+        copy_rv[k].start()
+    rv_recv[own_st, :] = rv_send[own_st, :]
+
+    for j in range(1, outer):
+        copy_hz[j].wait_recv()
+        fwd_z[j].start()
+    for j in range(1, outer):
+        fwd_z[j].wait_recv()
+        copy_mz[j].wait_recv()
+    copy_rs = [None]
+    for q in range(inner - 1, -1, -1):
+        target = xor(my_q, q)
+        dpart = pl.ds(aligned(target * dcols, dcols), dcols)
+        for s in range(half // 512):
+            cols = slice(s * 512, (s + 1) * 512)
+            total = dot_tn(hidden_z[0, :, dpart], mixed_z[0, :, cols])
+            for z in range(1, outer):
+                total = total + dot_tn(hidden_z[z, :, dpart], mixed_z[z, :, cols])
+            if q:
+                rs_send[q, :, cols] = total.astype(bf16)
+            else:
+                oproj[:, cols] = total
+        if q:
+            copy = remote(
+                rs_send.at[q], rs_recv.at[q], rs_s.at[q], rs_r.at[q], my_z * inner + target, tp
+            )
+            copy.start()
+            copy_rs.append(copy)
+
+    for k in range(1, n):
+        copy_rv[k].wait_recv()
+    head_l = iota((1, heads), 1)
+    grad_a = jnp.zeros((tokens, heads), f32)
+    for g in range(groups):
+        b_g = b_in[:, tile(g)]
+        gb = block_state[g]
+        for i in range(pairs_in_group):
+            pair = g * pairs_in_group + i
+            gy_t = gy[:, tile(pair)]
+            gyb = gy_t.astype(bf16)
+            x = scan_x[:, tile(pair)]
+            xf = x.astype(f32)
+            tail = spread(tail_s, pair)
+            later = rv_recv[tile(pair), :]
+            gx = dot_nn(mix_t[pair, :, 0:tokens], gyb * low_b)
+            gx = gx + dot_nn(mix_t[pair, :, tokens:2 * tokens], gyb * high_b)
+            gx = gx + dot_nt(b_g, later) * tail
+            oscan[:, tile(pair)] = gx.astype(bf16)
+            gb = gb + dot_nn((xf * tail).astype(bf16), later)
+            diff = gy_t * scan_out[:, tile(pair)] - xf * gx
+            sum_low = jnp.sum(jnp.where(low_lane, diff, 0.0), axis=1, keepdims=True)
+            sum_high = jnp.sum(jnp.where(low_lane, 0.0, diff), axis=1, keepdims=True)
+            grad_a = jnp.where(head_l == 2 * pair, sum_low, grad_a)
+            grad_a = jnp.where(head_l == 2 * pair + 1, sum_high, grad_a)
+        ob[:, tile(g)] = gb.astype(bf16)
+    gat_send[...] = jnp.zeros(gat_send.shape, f32)
+    gat_send[0:1, 0:heads] = jnp.sum(grad_a, axis=0, keepdims=True)
+    copy_gat = [None] + [
+        remote(gat_send, gat_recv.at[me], gat_s.at[k], gat_r.at[k], peers[k], tp)
+        for k in range(1, n)
+    ]
+    for k in far_first:
+        copy_gat[k].start()
+    gat_recv[me] = gat_send[...]
+
+    for j in range(outer):
+        for k in range(j * inner, (j + 1) * inner):
+            if k:
+                copy_h[k].wait_recv()
+        fwd_h[j].start()
+    for j in range(outer):
+        fwd_h[j].wait_recv()
+
+    def up_step(i, carry):
+        cols = pl.ds(aligned(i * 256, 256), 256)
+        for s in range(2):
+            lhs = h_full[s, :, cols]
+            grad_wg[s, cols, :] = dot_tn(lhs, gate_grad[...]).astype(bf16)
+            grad_wu[s, cols, :] = dot_tn(lhs, up_grad[...]).astype(bf16)
+        return carry
+
+    lax.fori_loop(0, half // 256, up_step, 0)
+    for i, (src, dst) in enumerate(((grad_wg, owg), (grad_wu, owu))):
+        stores.append(pltpu.make_async_copy(src, dst, out_sem.at[2 + i]))
+        stores[-1].start()
+
+    later_sum = dot_full(anti_f, grad_a)
+    for k in range(1, n):
+        copy_gat[k].wait_recv()
+    for b in range(n):
+        later_sum = later_sum + jnp.where(b > me, gat_recv[b, 0:1, 0:heads], 0.0)
+    odecay[...] = later_sum
+
+    for copy in copy_rs[1:]:
+        copy.wait_recv()
+    for q in range(1, inner):
+        oproj[...] += rs_recv[q].astype(f32)
+    for copies in (
+        copy_g, copy_h, copy_ret, copy_st, copy_rv, copy_tot, copy_gat, copy_mz, copy_hz, fwd_z,
+        copy_rs, fwd_g, fwd_h, px, [copy_gh],
+    ):
+        for copy in copies:
+            if copy is not None:
+                copy.wait_send()
+    for store in stores:
+        store.wait()
+
+
+def fused_body(
+    mixer_output, layer_cotangent, expert_choice, route_weight, gate_pre, up_pre,
+    w_gate, w_up, w_down, w_out, norm_gain, scan_in, gate_in, b_proj, c_proj,
+    log_decay, entry_state,
+):
+    n = lax.axis_size("sp")
+    outer = 4
+    inner = n // outer
+    tokens, width = mixer_output.shape
+    half = width // 2
+    rows, units = gate_pre.shape[1:]
+    cap = rows // n
+    heads = log_decay.shape[1]
+    channels = scan_in.shape[1]
+    state_rows = heads * HEAD_DIM
+    srows = state_rows // n
+    groups = b_proj.shape[1] // STATE
+    pairs = heads // 2
+    dchunk = width // outer
+    dcols = width // n
+    vm = pltpu.VMEM
+    dma = pltpu.SemaphoreType.DMA
+    wide = jax.ShapeDtypeStruct
+    vspec = pl.BlockSpec(memory_space=pltpu.VMEM)
+    aspec = pl.BlockSpec(memory_space=pl.ANY)
+    scratch = [
+        vm((tokens, half), bf16), vm((tokens, half), bf16),
+        vm((rows, units), bf16), vm((rows, units), bf16),
+        vm((2, half, units), bf16), vm((2, half, units), bf16),
+        vm((units, width), bf16), vm((channels, width), bf16),
+        vm((rows, half), bf16), vm((rows, half), bf16),
+        vm((2, rows, half), bf16), vm((2, rows, half), bf16),
+        vm((outer, rows // outer, half), bf16), vm((outer, rows // outer, half), bf16),
+        vm((rows, half), bf16), vm((rows, half), bf16),
+        vm((rows, units), bf16), vm((rows, units), bf16), vm((rows, units), bf16),
+        vm((tokens, rows), bf16),
+        vm((outer, tokens, channels), bf16), vm((outer, tokens, dchunk), bf16),
+        vm((outer, tokens, dchunk), bf16),
+        vm((inner, dcols, channels), bf16), vm((inner, dcols, channels), bf16),
+        vm((tokens, channels), f32), vm((tokens, channels), f32), vm((groups, tokens, 1), f32),
+        vm((tokens, channels), f32), vm((pairs, tokens, 2 * tokens), bf16),
+        vm((heads, tokens, tokens), f32), vm((tokens, heads), f32), vm((tokens, heads), f32),
+        vm((state_rows, STATE), bf16), vm((groups, tokens, STATE), f32),
+        vm((state_rows, STATE), bf16), vm((state_rows, STATE), bf16),
+        vm((state_rows, STATE), bf16), vm((state_rows, STATE), bf16),
+        vm((8, 128), f32), vm((n, 8, 128), f32), vm((8, 128), f32), vm((n, 8, 128), f32),
+        vm((2, half, units), bf16), vm((2, half, units), bf16), vm((2, units, half), bf16),
+        dma((8,)), dma((4,)),
+    ]
+    scratch += [dma((n,))] * 14
+    scratch += [dma((outer,))] * 8
+    scratch += [dma, dma]
+    scratch += [dma((outer,))] * 4
+    scratch += [dma((inner,))] * 2
+    outs = pl.pallas_call(
+        functools.partial(fused, (n, outer, cap)),
+        out_shape=(
+            wide((2, half, units), bf16), wide((2, half, units), bf16), wide((units, width), bf16),
+            wide((dcols, channels), f32), wide((tokens, channels), bf16),
+            wide((tokens, channels), bf16), wide((tokens, groups * STATE), bf16),
+            wide((tokens, groups * STATE), bf16), wide((tokens, heads), f32),
+        ),
+        in_specs=[vspec] * 11 + [aspec] * 8,
+        out_specs=(aspec,) * 3 + (vspec,) * 6,
+        scratch_shapes=scratch,
+        compiler_params=pltpu.CompilerParams(
+            collective_id=0, has_side_effects=True, vmem_limit_bytes=64 * 1024 * 1024 - 128 * 1024
+        ),
+        name="fused",
+    )(
+        expert_choice, expert_choice.T, route_weight.T, log_decay, log_decay.T,
+        norm_gain[None], scan_in, gate_in, b_proj, c_proj,
+        entry_state.reshape(state_rows, STATE),
+        layer_cotangent, mixer_output, gate_pre[0], up_pre[0],
+        w_gate.reshape(2, half, units), w_up.reshape(2, half, units), w_down[0], w_out,
+    )
+    gwg, gwu, gwd, proj, gscan, ggate, gb, gc, gdecay = outs
+    return (
+        gwg.reshape(1, width, units), gwu.reshape(1, width, units), gwd[None],
+        proj, gscan, ggate, gb, gc, gdecay,
+    )
 
 
 def entry_slots(expert_choice, expert_count, capacity):
@@ -327,4 +910,10 @@
         P("sp", "tp"),
         P("sp", "tp"),
     )
-    return jax.shard_map(body, mesh=mesh, in_specs=in_specs, out_specs=out_specs, check_vma=False)
+    def run(*args):
+        count = mesh.shape["sp"]
+        capacity = args[4].shape[1] // count
+        simple = mesh.shape["tp"] != 2 or count % 4 or count & (count - 1) or capacity % 16
+        return (body if simple else fused_body)(*args)
+
+    return jax.shard_map(run, mesh=mesh, in_specs=in_specs, out_specs=out_specs, check_vma=False)

time: 250 us -> 155 us (0.62)
  Pallas kernels: 0 us -> 137 us
  waiting for transfers between devices: 69.7 us -> 0 us
  matrix products: 47.4 us -> 0 us
  starting transfers between devices: 41.5 us -> 0 us
  blocking collectives: 36.7 us -> 0 us
  between operations: 16.3 us -> 0.66 us
  other arithmetic: 15.4 us -> 0 us
  local copies, waits for them, and re-layouts: 21.3 us -> 16.1 us
    pallas_call x0 -> x1, Pallas kernels: none -> 137 us  [fused_body(): pl.pallas_call(functools.partial(fused, (n, outer, cap)), out_shape=(wide...]
    all_to_all x7 -> x0, waiting for transfers between devices: 60.3 us -> none  [the longest x1 27.8 us: body(): lax.all_to_all(summed.reshape(expert_count, capacity, -1), 'sp', split_ax...]
    dot_general x27 -> x0, matrix products: 47.4 us -> none  [the longest x1 4.8 us: body(): jnp.einsum('rf,rd->fd', active, recv_grads, preferred_element_type=jnp.fl...]
    all_to_all x7 -> x0, starting transfers between devices: 41.4 us -> none  [the longest x2 10.1 us: exchange(): return lax.all_to_all(pieces, 'sp', split_axis=0, concat_axis=0, tiled=True)]
    all_to_all x1 -> x0, blocking collectives: 34.6 us -> none  [dispatch(): lax.all_to_all(rows.astype(jnp.bfloat16).reshape(expert_count, capacity,...]
    all_gather x3 -> x0, waiting for transfers between devices: 9.04 us -> none  [the longest x2 9.01 us: dispatch(): return lax.all_gather(arrived, 'tp', axis=1, tiled=True)]
    reduce_sum x7 -> x0, other arithmetic: 6.59 us -> none  [the longest x1 3.26 us: later_states(): sums = jnp.sum(weights[:, :, :, None] * dealt[None], axis=1)]
    unnamed x99 -> x25, local copies, waits for them, and re-layouts: 9.1 us -> 14.8 us
  transfers between devices with their start and end apart: 11 -> 0, of which waited for: 8 -> 0; matrix products, arithmetic and copies ran while one was open for 25% -> 0% of each run, Pallas kernels for 0% -> 0%
where the time goes in v1:
time: 155 us; the launch traced here: 154 us
  Pallas kernels  137 us (88%)
  local copies, waits for them, and re-layouts  16.1 us (10%)
    pallas_call x1, Pallas kernels, fused_body(): pl.pallas_call(functools.partial(fused, (n, outer, cap)), out_shape=(wide...  137 us
    unnamed x25, local copies, waits for them, and re-layouts  14.8 us

profile of v1, /device:TPU:0, one launch (start us, length us, event | category | flops | bytes accessed | tf_op | source)
XLA Modules:
  0.0 154.2 jit_solution(806191456081570739)
XLA Ops:
  0.6 1.3 broadcast_in_dim.6.gain
  1.9 1.4 copy.26.choice
  3.3 1.4 copy.27.decay
  4.8 137.5 %fused.1 = (bf16[2,1024,512]{2,1,0:T(8,128)(2,1)}, bf16[2,1024,512]{2,1,0:T(8,128)(2,1)}, bf16[512,2048]{1,0:T(8,128)(2,1)}, f32[128,1024]{1,0:T(8,128)}, bf16[1...) custom-call(s32[128,2]{1,0:T(8,128)} %copy.26.choice, ...), custom_call_target="tpu_custom_call" | custom-call | tf_op jit(solution)/shard_map/fused/pallas_call | solution.py:569
  142.2 1.5 copy.28
  143.8 0.0 copy-start.1
  143.8 3.2 %copy.37 = bf16[1,2048,512]{2,1,0:T(8,128)(2,1)} copy(bf16[1,2048,512]{2,1,0:T(8,128)(2,1)} %bitcast.17) | data formatting | bytes 4194304
  147.0 0.0 copy-done.1
  147.0 0.0 copy-start
  147.0 1.3 copy.38
  148.3 1.0 copy-done
  149.3 0.0 copy-start.2
  149.3 0.0 copy-start.4
  149.3 0.0 copy-start.3
  149.3 1.3 copy.39
  150.6 0.0 copy-done.2
  150.7 0.0 copy-start.6
  150.7 0.0 copy-start.5
  150.7 0.8 copy.40
  151.5 0.0 copy-done.4
  151.5 0.7 copy.41
  152.2 0.0 copy-done.3
  152.2 0.7 copy.42
  152.9 0.0 copy-done.6
  152.9 0.7 copy.43
  153.5 0.0 copy-done.5
  153.5 0.7 copy.44
Async XLA Ops:
  143.8 3.2 %copy-start.1 = (bf16[2,1024,512]{2,1,0:T(8,128)(2,1)S(1)}, bf16[2,1024,512]{2,1,0:T(8,128)(2,1)}, u32[]{:S(2)}) copy-start(bf16[2,1024,512]{2,1,0:T(8,128)(2,1)} %get-tuple-element.19) | copy-start | bytes 6291460
  147.0 2.3 %copy-start = (bf16[512,2048]{1,0:T(8,128)(2,1)S(1)}, bf16[512,2048]{1,0:T(8,128)(2,1)}, u32[]{:S(2)}) copy-start(bf16[512,2048]{1,0:T(8,128)(2,1)} %get-tuple-element.20) | copy-start | bytes 6291460
  149.3 1.4 copy-start.2
  149.3 2.2 %copy-start.4 = (bf16[128,1024]{1,0:T(8,128)(2,1)S(1)}, bf16[128,1024]{1,0:T(8,128)(2,1)}, u32[]{:S(2)}) copy-start(bf16[128,1024]{1,0:T(8,128)(2,1)} %get-tuple-element.49) | copy-start | bytes 786436
  149.3 2.9 %copy-start.3 = (bf16[128,1024]{1,0:T(8,128)(2,1)S(1)}, bf16[128,1024]{1,0:T(8,128)(2,1)}, u32[]{:S(2)}) copy-start(bf16[128,1024]{1,0:T(8,128)(2,1)} %get-tuple-element.50) | copy-start | bytes 786436
  150.7 2.2 %copy-start.6 = (bf16[128,512]{1,0:T(8,128)(2,1)S(1)}, bf16[128,512]{1,0:T(8,128)(2,1)}, u32[]{:S(2)}) copy-start(bf16[128,512]{1,0:T(8,128)(2,1)} %get-tuple-element.51) | copy-start | bytes 393220
  150.7 2.9 %copy-start.5 = (bf16[128,512]{1,0:T(8,128)(2,1)S(1)}, bf16[128,512]{1,0:T(8,128)(2,1)}, u32[]{:S(2)}) copy-start(bf16[128,512]{1,0:T(8,128)(2,1)} %get-tuple-element.52) | copy-start | bytes 393220

commit v2 on v1

--- a/solution.py
+++ b/solution.py
@@ -54,20 +54,24 @@
     return pl.multiple_of(value, unit)
 
 
+ORDER = (0, 2, 3, 1)
+PLAN = {'sent': (), 'forward': (), ('chunk', 0): (), ('chunk', 1): (), ('chunk', 2): (), ('chunk', 3): (), 'experts': ('hid0', 'mz0'), 'down': ('hid1', 'mz1'), 'combined': (), 'states': ('hid2', 'mz2'), 'inner': ('hid3', 'mz3'), 'later': ('proj',)}
+
+
 def fused(
     dims,
-    choice, choice_t, weight_t, decay, decay_t, gain, scan_x, gate_x, b_in, c_in, entry,
+    choice_t, weight_t, decay_t, gain, scan_x, gate_x, b_in, c_in, entry,
     cot_hbm, hid_hbm, gpre_hbm, upre_hbm, wg_hbm, wu_hbm, wd_hbm, wo_hbm,
     owg, owu, owd, oproj, oscan, ogate, ob, oc, odecay,
-    cot, hid, gpre, upre, wg, wu, wd, wo,
+    cot, hid_z, gpre, upre, wg, wu, wd, wo,
     send_g, send_h, g_full, h_full, part_send, part_recv, ret_send, ret_recv,
     active, gate_grad, up_grad, places_t,
     mixed_z, hidden, hidden_z, rs_send, rs_recv,
     scan_out, unit, inv_rms, gy, mix_t, decays, growth_s, tail_s, entry_b, block_state,
-    st_send, st_recv, rv_send, rv_recv, tot_send, tot_recv, gat_send, gat_recv,
+    st_send, st_recv, rv_send, rv_recv, tot_send, tot_recv, slot_recv, gat_send, gat_recv,
     grad_wg, grad_wu, grad_wd,
-    in_sem, out_sem, g_s, g_r, h_s, h_r, ret_s, ret_r, st_s, st_r, rv_s, rv_r,
-    tot_s, tot_r, gat_s, gat_r, fg_s, fg_r, fh_s, fh_r, px_s, px_r, mz_s, mz_r,
+    in_sem, out_sem, g_s, g_r, ret_s, ret_r, st_s, st_r, rv_s, rv_r,
+    tot_s, tot_r, gat_s, gat_r, fg_s, fg_r, fh_s, fh_r, px_s, px_r, sl_s, sl_r, mz_line, hid_line, h_s, h_r,
     gh_s, gh_r, hz_s, hz_r, fz_s, fz_r, rs_s, rs_r,
 ):
     n, outer, cap = dims
@@ -75,7 +79,7 @@
     tokens, half = cot.shape
     rows = n * cap
     zrows = inner * cap
-    heads = decay.shape[1]
+    heads = decay_t.shape[0]
     groups = b_in.shape[1] // STATE
     pairs_in_group = heads // groups // 2
     gwidth = pairs_in_group * 128
@@ -108,7 +112,7 @@
     own_cols = pl.ds(aligned(tp * half, half), half)
     loads = [
         pltpu.make_async_copy(cot_hbm.at[:, own_cols], cot, in_sem.at[0]),
-        pltpu.make_async_copy(hid_hbm.at[:, own_cols], hid, in_sem.at[1]),
+        pltpu.make_async_copy(hid_hbm.at[:, own_cols], hid_z.at[my_z], in_sem.at[1]),
         pltpu.make_async_copy(wd_hbm, wd, in_sem.at[2]),
         pltpu.make_async_copy(gpre_hbm, gpre, in_sem.at[3]),
         pltpu.make_async_copy(upre_hbm, upre, in_sem.at[4]),
@@ -130,19 +134,17 @@
     slot0_t = jnp.sum(jnp.where(first_t, base_t, 0.0), axis=0, keepdims=True)
     slot1_t = jnp.sum(jnp.where(second_t, base_t, 0.0), axis=0, keepdims=True)
 
-    expert_l = iota((tokens, n), 1)
-    first = choice[:, 0:1] == expert_l
-    second = choice[:, 1:2] == expert_l
-    named = jnp.where(first | second, 1.0, 0.0).astype(bf16)
-    before = jnp.where(row_id > col_id, 1.0, 0.0).astype(bf16)
-    base = dot_nn(before, named) + (cap * expert_l).astype(f32)
-    slot0 = jnp.sum(jnp.where(first, base, 0.0), axis=1, keepdims=True)
-    slot1 = jnp.sum(jnp.where(second, base, 0.0), axis=1, keepdims=True)
+    def column(row):
+        return jnp.sum(jnp.where(row_id == col_id, row, 0.0), axis=1, keepdims=True)
+
+    slot0, slot1 = column(slot0_t), column(slot1_t)
     slot_l = iota((tokens, rows), 1).astype(f32)
     places_t[...] = jnp.where((slot_l == slot0) | (slot_l == slot1), 1.0, 0.0).astype(bf16)
 
+    slot_recv[my_z] = jnp.zeros(slot_recv.shape[1:], f32)
+    slot_recv[my_z, 0:1, :] = slot0_t
+    slot_recv[my_z, 1:2, :] = slot1_t
     loads[0].wait()
-    loads[1].wait()
     for z in range(outer):
         part = slice(z * zrows, (z + 1) * zrows)
         slot_s = (iota((zrows, tokens), 0) + z * zrows).astype(f32)
@@ -154,9 +156,49 @@
             axis=1, keepdims=True,
         )
         send_g[part, :] = (dot_nn(places, cot[...]) * scale).astype(bf16)
-        send_h[part, :] = dot_nn(places, hid[...]).astype(bf16)
 
     pl.semaphore_wait(barrier, n)
+
+    def line(buf, sems):
+        def up(s):
+            block = (my_z - s + outer) % outer
+            return remote(
+                buf.at[block], buf.at[block], sems.at[0, s], sems.at[1, s], (me + inner) % n, tp
+            )
+
+        def down(s):
+            block = (my_z + s) % outer
+            return remote(
+                buf.at[block], buf.at[block], sems.at[2, s], sems.at[3, s],
+                (me - inner + n) % n, tp,
+            )
+
+        def send(s, drain=False):
+            @pl.when((my_z >= s) & (my_z < outer - 1))
+            def _():
+                up(s).wait_send() if drain else up(s).start()
+
+            @pl.when((my_z + s < outer) & (my_z > 0))
+            def _():
+                down(s).wait_send() if drain else down(s).start()
+
+        def take(s):
+            @pl.when(my_z > s)
+            def _():
+                up(s).wait_recv()
+
+            @pl.when(my_z + s + 1 < outer)
+            def _():
+                down(s).wait_recv()
+
+        return send, take
+
+    send_hid, take_hid = line(hid_z, hid_line)
+    send_mz, take_mz = line(mixed_z, mz_line)
+
+    def at(point):
+        for step in PLAN[point]:
+            steps[step]()
 
     def all_to_all(send, recv, size, s, r):
         mine = rowblock(me, size)
@@ -167,7 +209,6 @@
 
     own_rows = rowblock(me, cap)
     copy_g = all_to_all(send_g, g_full.at[tp], cap, g_s, g_r)
-    copy_h = all_to_all(send_h, h_full.at[tp], cap, h_s, h_r)
     copy_ret = all_to_all(ret_send, ret_recv, cap, ret_s, ret_r)
     copy_st = all_to_all(st_send, st_recv, srows, st_s, st_r)
     copy_rv = all_to_all(rv_send, rv_recv, srows, rv_s, rv_r)
@@ -175,13 +216,91 @@
     for k in far_first:
         copy_g[k].start()
     g_full[tp, own_rows, :] = send_g[own_rows, :]
-    h_full[tp, own_rows, :] = send_h[own_rows, :]
+
+    copy_rs = [None]
+
+    def output_projection():
+        for j in range(1, outer):
+            copy_hz[j].wait_recv()
+            fwd_z[j].start()
+        for j in range(1, outer):
+            fwd_z[j].wait_recv()
+        for q in range(inner - 1, -1, -1):
+            target = xor(my_q, q)
+            dpart = pl.ds(aligned(target * dcols, dcols), dcols)
+            for s in range(half // 512):
+                cols = slice(s * 512, (s + 1) * 512)
+                total = dot_tn(hidden_z[0, :, dpart], mixed_z[0, :, cols])
+                for z in range(1, outer):
+                    total = total + dot_tn(hidden_z[z, :, dpart], mixed_z[z, :, cols])
+                if q:
+                    rs_send[q, :, cols] = total.astype(bf16)
+                else:
+                    oproj[:, cols] = total
+            if q:
+                copy = remote(
+                    rs_send.at[q], rs_recv.at[q], rs_s.at[q], rs_r.at[q], my_z * inner + target, tp
+                )
+                copy.start()
+                copy_rs.append(copy)
+
+    copy_h = []
+
+    def hidden_block(b, j):
+        slot_h = (iota((zrows, tokens), 0) + my_z * zrows).astype(f32)
+        found = (slot_h == slot_recv[b, 0:1, :]) | (slot_h == slot_recv[b, 1:2, :])
+        places = jnp.where(found, 1.0, 0.0).astype(bf16)
+        send_h[j] = dot_nn(places, hid_z[b]).astype(bf16)
+        dest = pl.ds(aligned((b * inner + my_q) * cap, cap), cap)
+        for q in range(1, inner):
+            target = xor(my_q, q)
+            copy = remote(
+                send_h.at[j, rowblock(target, cap)], h_full.at[tp, dest],
+                h_s.at[j, q], h_r.at[j, q], my_z * inner + target, tp,
+            )
+            copy.start()
+            copy_h.append(copy)
+        h_full[tp, dest, :] = send_h[j, rowblock(my_q, cap), :]
+
+    def hidden_own():
+        loads[1].wait()
+        send_hid(0)
+        hidden_block(my_z, 0)
+
+    def hidden_send():
+        loads[1].wait()
+        send_hid(0)
+
+    def hidden_rest():
+        take_hid(outer - 2)
+        for j in range(1, outer):
+            copy_sl[j].wait_recv()
+        for j in range(1, outer):
+            hidden_block(xor(my_z, j), j)
+
+    def pass_on(send, take, s):
+        take(s - 1)
+        send(s)
+
+    steps = {
+        "hid0": hidden_own,
+        "hid0s": hidden_send,
+        "hid0b": lambda: hidden_block(my_z, 0),
+        "hid1": lambda: pass_on(send_hid, take_hid, 1),
+        "hid2": lambda: pass_on(send_hid, take_hid, 2),
+        "hid3": hidden_rest,
+        "mz0": lambda: send_mz(0),
+        "mz1": lambda: pass_on(send_mz, take_mz, 1),
+        "mz2": lambda: pass_on(send_mz, take_mz, 2),
+        "mz3": lambda: take_mz(outer - 2),
+        "proj": output_projection,
+    }
 
     causal = row_id >= col_id
     causal_f = jnp.where(causal, 1.0, 0.0)
     anti_f = jnp.where(row_id <= col_id, 1.0, 0.0)
-    cum = dot_full(causal_f, decay[...])
     cum_t = dot_full(decay_t[...], anti_f)
+    cum = cum_t.T
     growth_s[...] = jnp.exp(cum)
     tail_s[...] = jnp.exp(cum[tokens - 1:tokens, :] - cum)
     tot_send[...] = jnp.zeros(tot_send.shape, f32)
@@ -193,6 +312,16 @@
     ]
     for k in far_first:
         copy_tot[k].start()
+    copy_sl = [None] + [
+        remote(
+            slot_recv.at[my_z], slot_recv.at[my_z], sl_s.at[j], sl_r.at[j],
+            xor(my_z, j) * inner + my_q, tp,
+        )
+        for j in range(1, outer)
+    ]
+    for j in range(1, outer):
+        copy_sl[j].start()
+    at("sent")
     lane = iota((1, 128), 1)
     low_lane = lane < HEAD_DIM
     low = jnp.where(low_lane, 1.0, 0.0)
@@ -205,6 +334,9 @@
 
     def tile(index):
         return slice(index * 128, (index + 1) * 128)
+
+    def gain_row(index):
+        return gain[index:index + 1, :].astype(f32)
 
     def group_cols(g):
         return slice(g * gwidth, (g + 1) * gwidth)
@@ -242,15 +374,9 @@
             cols = tile(g * pairs_in_group + i)
             flat = value * inv
             unit[:, cols] = flat
-            mixed_z[my_z, :, cols] = (flat * gain[:, cols].astype(f32)).astype(bf16)
-
-    copy_mz = [None] + [
-        remote(
-            mixed_z.at[my_z], mixed_z.at[my_z], mz_s.at[j], mz_r.at[j],
-            xor(my_z, j) * inner + my_q, tp,
-        )
-        for j in range(1, outer)
-    ]
+            mixed_z[my_z, :, cols] = (flat * gain_row(g * pairs_in_group + i)).astype(bf16)
+
+    at("forward")
 
     for i in range(2, 7):
         loads[i].wait()
@@ -264,7 +390,7 @@
             remote(h_full.at[tp, zpart], h_full.at[tp, zpart], fh_s.at[j], fh_r.at[j], me, other)
         )
         px.append(remote(part_send.at[j], part_recv.at[j], px_s.at[j], px_r.at[j], me, other))
-    for j in range(outer):
+    for count, j in enumerate(ORDER):
         for k in range(j * inner, (j + 1) * inner):
             if k:
                 copy_g[k].wait_recv()
@@ -296,9 +422,9 @@
         for k in range(j * inner, (j + 1) * inner):
             if k:
                 copy_ret[k].start()
-
-    for k in far_first:
-        copy_h[k].start()
+        at(("chunk", count))
+
+    at("experts")
 
     def down_step(i, carry):
         cols = pl.ds(aligned(i * 256, 256), 256)
@@ -314,6 +440,7 @@
     stores[0].start()
     stores[1].start()
 
+    at("down")
     for k in range(1, n):
         copy_ret[k].wait_recv()
     moe = dot_nn(places_t[...], ret_recv[...])
@@ -344,6 +471,7 @@
         )
     for j in range(outer - 1, 0, -1):
         copy_hz[j].start()
+    at("combined")
 
     for g in range(groups):
         c_g = c_in[:, tile(g)]
@@ -351,7 +479,13 @@
         gm = dot_nt(hidden[0], wo[gcols, 0:dchunk])
         for i in range(1, outer):
             gm = gm + dot_nt(hidden[i], wo[gcols, i * dchunk:(i + 1) * dchunk])
-        gu = gm * gain[:, gcols].astype(f32)
+        gu = jnp.concatenate(
+            [
+                gm[:, tile(i)] * gain_row(g * pairs_in_group + i)
+                for i in range(pairs_in_group)
+            ],
+            axis=1,
+        )
         flat = unit[:, gcols]
         mean = jnp.sum(gu * flat, axis=1, keepdims=True) * (1.0 / gwidth)
         gg = inv_rms[g] * (gu - flat * mean)
@@ -370,8 +504,7 @@
     for k in far_first:
         copy_st[k].start()
     st_recv[own_st, :] = st_send[own_st, :]
-    for j in range(outer - 1, 0, -1):
-        copy_mz[j].start()
+    at("states")
 
     for g in range(groups):
         b_g, c_g = b_in[:, tile(g)], c_in[:, tile(g)]
@@ -390,6 +523,8 @@
         oc[:, tile(g)] = (gc + dot_nn(gwb, b_g)).astype(bf16)
         block_state[g] = dot_tn(gwb, c_g)
 
+    at("inner")
+
     for k in range(1, n):
         copy_tot[k].wait_recv()
         copy_st[k].wait_recv()
@@ -406,32 +541,7 @@
     for k in far_first:
         copy_rv[k].start()
     rv_recv[own_st, :] = rv_send[own_st, :]
-
-    for j in range(1, outer):
-        copy_hz[j].wait_recv()
-        fwd_z[j].start()
-    for j in range(1, outer):
-        fwd_z[j].wait_recv()
-        copy_mz[j].wait_recv()
-    copy_rs = [None]
-    for q in range(inner - 1, -1, -1):
-        target = xor(my_q, q)
-        dpart = pl.ds(aligned(target * dcols, dcols), dcols)
-        for s in range(half // 512):
-            cols = slice(s * 512, (s + 1) * 512)
-            total = dot_tn(hidden_z[0, :, dpart], mixed_z[0, :, cols])
-            for z in range(1, outer):
-                total = total + dot_tn(hidden_z[z, :, dpart], mixed_z[z, :, cols])
-            if q:
-                rs_send[q, :, cols] = total.astype(bf16)
-            else:
-                oproj[:, cols] = total
-        if q:
-            copy = remote(
-                rs_send.at[q], rs_recv.at[q], rs_s.at[q], rs_r.at[q], my_z * inner + target, tp
-            )
-            copy.start()
-            copy_rs.append(copy)
+    at("later")
 
     for k in range(1, n):
         copy_rv[k].wait_recv()
@@ -459,8 +569,8 @@
             grad_a = jnp.where(head_l == 2 * pair, sum_low, grad_a)
             grad_a = jnp.where(head_l == 2 * pair + 1, sum_high, grad_a)
         ob[:, tile(g)] = gb.astype(bf16)
-    gat_send[...] = jnp.zeros(gat_send.shape, f32)
-    gat_send[0:1, 0:heads] = jnp.sum(grad_a, axis=0, keepdims=True)
+    grad_t = grad_a.T
+    gat_send[...] = jnp.broadcast_to(jnp.sum(grad_t, axis=1, keepdims=True), gat_send.shape)
     copy_gat = [None] + [
         remote(gat_send, gat_recv.at[me], gat_s.at[k], gat_r.at[k], peers[k], tp)
         for k in range(1, n)
@@ -470,9 +580,8 @@
     gat_recv[me] = gat_send[...]
 
     for j in range(outer):
-        for k in range(j * inner, (j + 1) * inner):
-            if k:
-                copy_h[k].wait_recv()
+        for copy in copy_h[j * (inner - 1):(j + 1) * (inner - 1)]:
+            copy.wait_recv()
         fwd_h[j].start()
     for j in range(outer):
         fwd_h[j].wait_recv()
@@ -490,11 +599,11 @@
         stores.append(pltpu.make_async_copy(src, dst, out_sem.at[2 + i]))
         stores[-1].start()
 
-    later_sum = dot_full(anti_f, grad_a)
+    later_sum = dot_full(grad_t, causal_f)
     for k in range(1, n):
         copy_gat[k].wait_recv()
     for b in range(n):
-        later_sum = later_sum + jnp.where(b > me, gat_recv[b, 0:1, 0:heads], 0.0)
+        later_sum = later_sum + jnp.where(b > me, gat_recv[b, :, 0:1], 0.0)
     odecay[...] = later_sum
 
     for copy in copy_rs[1:]:
@@ -502,14 +611,48 @@
     for q in range(1, inner):
         oproj[...] += rs_recv[q].astype(f32)
     for copies in (
-        copy_g, copy_h, copy_ret, copy_st, copy_rv, copy_tot, copy_gat, copy_mz, copy_hz, fwd_z,
+        copy_g, copy_h, copy_ret, copy_st, copy_rv, copy_tot, copy_gat, copy_sl, copy_hz, fwd_z,
         copy_rs, fwd_g, fwd_h, px, [copy_gh],
     ):
         for copy in copies:
             if copy is not None:
                 copy.wait_send()
+    for s in range(outer - 1):
+        send_hid(s, drain=True)
+        send_mz(s, drain=True)
     for store in stores:
         store.wait()
+
+
+def pass_through(count, *refs):
+    ins, outs, held = refs[:count], refs[count:2 * count], refs[2 * count:3 * count]
+    in_sem, out_sem = refs[3 * count:]
+    reads = [pltpu.make_async_copy(ins[i], held[i], in_sem.at[i]) for i in range(count)]
+    writes = [pltpu.make_async_copy(held[i], outs[i], out_sem.at[i]) for i in range(count)]
+    for read in reads:
+        read.start()
+    for read, write in zip(reads, writes):
+        read.wait()
+        write.start()
+    for write in writes:
+        write.wait()
+
+
+def hand_over(arrays):
+    count = len(arrays)
+    pieces = []
+    for array in arrays:
+        pieces.append(jax.ShapeDtypeStruct(array.shape, array.dtype))
+    aspec = pl.BlockSpec(memory_space=pl.ANY)
+    return pl.pallas_call(
+        functools.partial(pass_through, count),
+        out_shape=tuple(pieces),
+        in_specs=[aspec] * count,
+        out_specs=(aspec,) * count,
+        scratch_shapes=[pltpu.VMEM(p.shape, p.dtype) for p in pieces]
+        + [pltpu.SemaphoreType.DMA((count,))] * 2,
+        name="hand_over",
+    )(*arrays)
 
 
 def fused_body(
@@ -538,11 +681,11 @@
     vspec = pl.BlockSpec(memory_space=pltpu.VMEM)
     aspec = pl.BlockSpec(memory_space=pl.ANY)
     scratch = [
-        vm((tokens, half), bf16), vm((tokens, half), bf16),
+        vm((tokens, half), bf16), vm((outer, tokens, half), bf16),
         vm((rows, units), bf16), vm((rows, units), bf16),
         vm((2, half, units), bf16), vm((2, half, units), bf16),
         vm((units, width), bf16), vm((channels, width), bf16),
-        vm((rows, half), bf16), vm((rows, half), bf16),
+        vm((rows, half), bf16), vm((outer, rows // outer, half), bf16),
         vm((2, rows, half), bf16), vm((2, rows, half), bf16),
         vm((outer, rows // outer, half), bf16), vm((outer, rows // outer, half), bf16),
         vm((rows, half), bf16), vm((rows, half), bf16),
@@ -557,12 +700,14 @@
         vm((state_rows, STATE), bf16), vm((groups, tokens, STATE), f32),
         vm((state_rows, STATE), bf16), vm((state_rows, STATE), bf16),
         vm((state_rows, STATE), bf16), vm((state_rows, STATE), bf16),
-        vm((8, 128), f32), vm((n, 8, 128), f32), vm((8, 128), f32), vm((n, 8, 128), f32),
+        vm((8, 128), f32), vm((n, 8, 128), f32), vm((outer, 8, tokens), f32),
+        vm((heads, 128), f32), vm((n, heads, 128), f32),
         vm((2, half, units), bf16), vm((2, half, units), bf16), vm((2, units, half), bf16),
         dma((8,)), dma((4,)),
     ]
-    scratch += [dma((n,))] * 14
+    scratch += [dma((n,))] * 12
     scratch += [dma((outer,))] * 8
+    scratch += [dma((4, outer)), dma((4, outer)), dma((outer, inner)), dma((outer, inner))]
     scratch += [dma, dma]
     scratch += [dma((outer,))] * 4
     scratch += [dma((inner,))] * 2
@@ -572,9 +717,9 @@
             wide((2, half, units), bf16), wide((2, half, units), bf16), wide((units, width), bf16),
             wide((dcols, channels), f32), wide((tokens, channels), bf16),
             wide((tokens, channels), bf16), wide((tokens, groups * STATE), bf16),
-            wide((tokens, groups * STATE), bf16), wide((tokens, heads), f32),
+            wide((tokens, groups * STATE), bf16), wide((heads, tokens), f32),
         ),
-        in_specs=[vspec] * 11 + [aspec] * 8,
+        in_specs=[vspec] * 9 + [aspec] * 8,
         out_specs=(aspec,) * 3 + (vspec,) * 6,
         scratch_shapes=scratch,
         compiler_params=pltpu.CompilerParams(
@@ -582,16 +727,16 @@
         ),
         name="fused",
     )(
-        expert_choice, expert_choice.T, route_weight.T, log_decay, log_decay.T,
-        norm_gain[None], scan_in, gate_in, b_proj, c_proj,
+        expert_choice.T, route_weight.T, log_decay.T,
+        norm_gain.reshape(channels // 128, 128), scan_in, gate_in, b_proj, c_proj,
         entry_state.reshape(state_rows, STATE),
         layer_cotangent, mixer_output, gate_pre[0], up_pre[0],
         w_gate.reshape(2, half, units), w_up.reshape(2, half, units), w_down[0], w_out,
     )
-    gwg, gwu, gwd, proj, gscan, ggate, gb, gc, gdecay = outs
+    gwg, gwu, gwd, proj, gscan, ggate, gb, gc, gdecay = hand_over(outs)
     return (
         gwg.reshape(1, width, units), gwu.reshape(1, width, units), gwd[None],
-        proj, gscan, ggate, gb, gc, gdecay,
+        proj, gscan, ggate, gb, gc, gdecay.T,
     )
 
 

time: 155 us -> 123 us (0.79)
  local copies, waits for them, and re-layouts: 16.1 us -> 0 us
  Pallas kernels: 137 us -> 122 us
    pallas_call x1, Pallas kernels: 137 us -> 116 us  [fused_body(): pl.pallas_call(functools.partial(fused, (n, outer, cap)), out_shape=(wide...]
    unnamed x25 -> x0, local copies, waits for them, and re-layouts: 14.8 us -> none
    pallas_call x0 -> x1, Pallas kernels: none -> 5.51 us  [hand_over(): pl.pallas_call(functools.partial(pass_through, count), out_shape=tuple(pi...]
where the time goes in v2:
time: 123 us
  Pallas kernels  122 us (99%)
    pallas_call x1, Pallas kernels, fused_body(): pl.pallas_call(functools.partial(fused, (n, outer, cap)), out_shape=(wide...  116 us
    pallas_call x1, Pallas kernels, hand_over(): pl.pallas_call(functools.partial(pass_through, count), out_shape=tuple(pi...  5.51 us

profile of v2, /device:TPU:0, one launch (start us, length us, event | category | flops | bytes accessed | tf_op | source)
XLA Modules:
  0.0 122.7 jit_solution(4697807013782707100)
XLA Ops:
  0.6 116.4 %fused.1 = (bf16[2,1024,512]{2,1,0:T(8,128)(2,1)}, bf16[2,1024,512]{2,1,0:T(8,128)(2,1)}, bf16[512,2048]{1,0:T(8,128)(2,1)}, f32[128,1024]{1,0:T(8,128)}, bf16[1...) custom-call(s32[2,128]{1,0:T(2,128)} %bitcast.22, ...), custom_call_target="tpu_custom_call" | custom-call | tf_op jit(solution)/shard_map/fused/pallas_call | solution.py:714
  117.1 5.5 %hand_over.1 = (bf16[2,1024,512]{2,1,0:T(8,128)(2,1)}, bf16[2,1024,512]{2,1,0:T(8,128)(2,1)}, bf16[512,2048]{1,0:T(8,128)(2,1)}, f32[128,1024]{1,0:T(8,128)}, bf...) custom-call(bf16[2,1024,512]{2,1,0:T(8,128)(2,1)} %get-tuple-element, ...), custom_call_target="tpu_custom_call" | custom-call | tf_op jit(solution)/shard_map/hand_over/pallas_call | solution.py:647

commit v3 on v2

--- a/solution.py
+++ b/solution.py
@@ -54,29 +54,29 @@
     return pl.multiple_of(value, unit)
 
 
-ORDER = (0, 2, 3, 1)
-PLAN = {'sent': (), 'forward': (), ('chunk', 0): (), ('chunk', 1): (), ('chunk', 2): (), ('chunk', 3): (), 'experts': ('hid0', 'mz0'), 'down': ('hid1', 'mz1'), 'combined': (), 'states': ('hid2', 'mz2'), 'inner': ('hid3', 'mz3'), 'later': ('proj',)}
+PLAN = {'sent': (), ('chunk', 0): (), ('chunk', 1): ('cot2', 'hid0'), ('chunk', 2): ('cot3', 'hid1'), ('chunk', 3): (), 'forward': ('cot1',), 'experts': ('hid2', 'mz0'), 'down': ('hid3', 'mz1'), 'combined': (), 'states': ('mz2',), 'inner': ('mz3',), 'later': ('proj',), 'final': ()}
 
 
 def fused(
     dims,
-    choice_t, weight_t, decay_t, gain, scan_x, gate_x, b_in, c_in, entry,
+    choice_t, weight_t, decay_t, gain, scan_hbm, gate_hbm, b_hbm, c_hbm, entry_hbm,
     cot_hbm, hid_hbm, gpre_hbm, upre_hbm, wg_hbm, wu_hbm, wd_hbm, wo_hbm,
-    owg, owu, owd, oproj, oscan, ogate, ob, oc, odecay,
-    cot, hid_z, gpre, upre, wg, wu, wd, wo,
+    owg, owu, owd, proj_hbm, oscan_hbm, ogate_hbm, ob_hbm, oc_hbm, odecay,
+    scan_x, gate_x, b_in, c_in, entry, oproj, oscan, ogate, ob, oc,
+    cot_z, hid_z, gpre, upre, wg, wu, wd, wo,
     send_g, send_h, g_full, h_full, part_send, part_recv, ret_send, ret_recv,
     active, gate_grad, up_grad, places_t,
     mixed_z, hidden, hidden_z, rs_send, rs_recv,
     scan_out, unit, inv_rms, gy, mix_t, decays, growth_s, tail_s, entry_b, block_state,
     st_send, st_recv, rv_send, rv_recv, tot_send, tot_recv, slot_recv, gat_send, gat_recv,
     grad_wg, grad_wu, grad_wd,
-    in_sem, out_sem, g_s, g_r, ret_s, ret_r, st_s, st_r, rv_s, rv_r,
-    tot_s, tot_r, gat_s, gat_r, fg_s, fg_r, fh_s, fh_r, px_s, px_r, sl_s, sl_r, mz_line, hid_line, h_s, h_r,
+    in_sem, out_sem, ret_s, ret_r, st_s, st_r, rv_s, rv_r,
+    tot_s, tot_r, gat_s, gat_r, fg_s, fg_r, fh_s, fh_r, px_s, px_r, sl_s, sl_r, mz_line, hid_line, cot_line, h_s, h_r, g_s, g_r,
     gh_s, gh_r, hz_s, hz_r, fz_s, fz_r, rs_s, rs_r,
 ):
     n, outer, cap = dims
     inner = n // outer
-    tokens, half = cot.shape
+    tokens, half = cot_z.shape[1:]
     rows = n * cap
     zrows = inner * cap
     heads = decay_t.shape[0]
@@ -111,7 +111,7 @@
 
     own_cols = pl.ds(aligned(tp * half, half), half)
     loads = [
-        pltpu.make_async_copy(cot_hbm.at[:, own_cols], cot, in_sem.at[0]),
+        pltpu.make_async_copy(cot_hbm.at[:, own_cols], cot_z.at[my_z], in_sem.at[0]),
         pltpu.make_async_copy(hid_hbm.at[:, own_cols], hid_z.at[my_z], in_sem.at[1]),
         pltpu.make_async_copy(wd_hbm, wd, in_sem.at[2]),
         pltpu.make_async_copy(gpre_hbm, gpre, in_sem.at[3]),
@@ -120,7 +120,21 @@
         pltpu.make_async_copy(wu_hbm, wu, in_sem.at[6]),
         pltpu.make_async_copy(wo_hbm, wo, in_sem.at[7]),
     ]
-    for load in loads:
+    pairs_of_refs = (
+        (b_hbm, b_in), (c_hbm, c_in), (scan_hbm, scan_x), (entry_hbm, entry), (gate_hbm, gate_x),
+    )
+    mixer_loads = [
+        pltpu.make_async_copy(src, dst, in_sem.at[8 + i])
+        for i, (src, dst) in enumerate(pairs_of_refs)
+    ]
+    stores = []
+
+    def store(src, dst):
+        copy = pltpu.make_async_copy(src, dst, out_sem.at[len(stores)])
+        copy.start()
+        stores.append(copy)
+
+    for load in loads[:2] + mixer_loads + loads[2:]:
         load.start()
 
     expert_s = iota((n, tokens), 0)
@@ -144,19 +158,8 @@
     slot_recv[my_z] = jnp.zeros(slot_recv.shape[1:], f32)
     slot_recv[my_z, 0:1, :] = slot0_t
     slot_recv[my_z, 1:2, :] = slot1_t
+    slot_recv[my_z, 2:4, :] = weight_t[...]
     loads[0].wait()
-    for z in range(outer):
-        part = slice(z * zrows, (z + 1) * zrows)
-        slot_s = (iota((zrows, tokens), 0) + z * zrows).astype(f32)
-        in_first = slot_s == slot0_t
-        in_second = slot_s == slot1_t
-        places = jnp.where(in_first | in_second, 1.0, 0.0).astype(bf16)
-        scale = jnp.sum(
-            jnp.where(in_first, weight_t[0:1, :], 0.0) + jnp.where(in_second, weight_t[1:2, :], 0.0),
-            axis=1, keepdims=True,
-        )
-        send_g[part, :] = (dot_nn(places, cot[...]) * scale).astype(bf16)
-
     pl.semaphore_wait(barrier, n)
 
     def line(buf, sems):
@@ -195,6 +198,7 @@
 
     send_hid, take_hid = line(hid_z, hid_line)
     send_mz, take_mz = line(mixed_z, mz_line)
+    send_cot, take_cot = line(cot_z, cot_line)
 
     def at(point):
         for step in PLAN[point]:
@@ -208,14 +212,19 @@
         ]
 
     own_rows = rowblock(me, cap)
-    copy_g = all_to_all(send_g, g_full.at[tp], cap, g_s, g_r)
-    copy_ret = all_to_all(ret_send, ret_recv, cap, ret_s, ret_r)
     copy_st = all_to_all(st_send, st_recv, srows, st_s, st_r)
     copy_rv = all_to_all(rv_send, rv_recv, srows, rv_s, rv_r)
     far_first = list(range(n - 1, 0, -1))
-    for k in far_first:
-        copy_g[k].start()
-    g_full[tp, own_rows, :] = send_g[own_rows, :]
+    copy_sl = [None] + [
+        remote(
+            slot_recv.at[my_z], slot_recv.at[my_z], sl_s.at[j], sl_r.at[j],
+            xor(my_z, j) * inner + my_q, tp,
+        )
+        for j in range(1, outer)
+    ]
+    send_cot(0)
+    for j in range(1, outer):
+        copy_sl[j].start()
 
     copy_rs = [None]
 
@@ -244,57 +253,111 @@
                 copy.start()
                 copy_rs.append(copy)
 
-    copy_h = []
-
-    def hidden_block(b, j):
+    def plane_dest(b):
+        return pl.ds(aligned((b * inner + my_q) * cap, cap), cap)
+
+    def plane_copy(send, full, sems, b, q):
+        target = xor(my_q, q)
+        return remote(
+            send.at[b, rowblock(target, cap)], full.at[tp, plane_dest(b)],
+            sems[0].at[b, q], sems[1].at[b, q], my_z * inner + target, tp,
+        )
+
+    def hidden_copy(b, q):
+        return plane_copy(send_h, h_full, (h_s, h_r), b, q)
+
+    def cot_copy(b, q):
+        return plane_copy(send_g, g_full, (g_s, g_r), b, q)
+
+    def deal(b, source, send, full, copy, weighted):
         slot_h = (iota((zrows, tokens), 0) + my_z * zrows).astype(f32)
-        found = (slot_h == slot_recv[b, 0:1, :]) | (slot_h == slot_recv[b, 1:2, :])
-        places = jnp.where(found, 1.0, 0.0).astype(bf16)
-        send_h[j] = dot_nn(places, hid_z[b]).astype(bf16)
-        dest = pl.ds(aligned((b * inner + my_q) * cap, cap), cap)
-        for q in range(1, inner):
-            target = xor(my_q, q)
-            copy = remote(
-                send_h.at[j, rowblock(target, cap)], h_full.at[tp, dest],
-                h_s.at[j, q], h_r.at[j, q], my_z * inner + target, tp,
+        in_first = slot_h == slot_recv[b, 0:1, :]
+        in_second = slot_h == slot_recv[b, 1:2, :]
+        places = jnp.where(in_first | in_second, 1.0, 0.0).astype(bf16)
+        rows_b = dot_nn(places, source[b])
+        if weighted:
+            rows_b = rows_b * jnp.sum(
+                jnp.where(in_first, slot_recv[b, 2:3, :], 0.0)
+                + jnp.where(in_second, slot_recv[b, 3:4, :], 0.0),
+                axis=1, keepdims=True,
             )
-            copy.start()
-            copy_h.append(copy)
-        h_full[tp, dest, :] = send_h[j, rowblock(my_q, cap), :]
+        send[b] = rows_b.astype(bf16)
+        for q in range(inner - 1, 0, -1):
+            copy(b, q).start()
+        full[tp, plane_dest(b), :] = send[b, rowblock(my_q, cap), :]
+
+    def hidden_block(b):
+        deal(b, hid_z, send_h, h_full, hidden_copy, False)
+
+    def cot_block(b):
+        deal(b, cot_z, send_g, g_full, cot_copy, True)
+
+    def at_distance(distance, action):
+        @pl.when(my_z >= distance)
+        def _():
+            action((my_z - distance + outer) % outer)
+
+        @pl.when(my_z + distance < outer)
+        def _():
+            action((my_z + distance) % outer)
+
+    def cot_next(s):
+        if s == 1:
+            for j in range(1, outer):
+                copy_sl[j].wait_recv()
+        take_cot(s - 1)
+        if s < outer - 1:
+            send_cot(s)
+        at_distance(s, cot_block)
 
     def hidden_own():
         loads[1].wait()
         send_hid(0)
-        hidden_block(my_z, 0)
+        hidden_block(my_z)
 
     def hidden_send():
         loads[1].wait()
         send_hid(0)
 
-    def hidden_rest():
-        take_hid(outer - 2)
-        for j in range(1, outer):
-            copy_sl[j].wait_recv()
-        for j in range(1, outer):
-            hidden_block(xor(my_z, j), j)
+    def hidden_next(s):
+        take_hid(s - 1)
+        if s < outer - 1:
+            send_hid(s)
+        at_distance(s, hidden_block)
+
+    forwarded = []
+
+    def forward_hidden(j):
+        for q in range(1, inner):
+            hidden_copy(xor(my_z, j), q).wait_recv()
+        fwd_h[j].start()
+        forwarded.append(j)
 
     def pass_on(send, take, s):
         take(s - 1)
         send(s)
 
     steps = {
+        "cot1": lambda: cot_next(1),
+        "cot2": lambda: cot_next(2),
+        "cot3": lambda: cot_next(3),
         "hid0": hidden_own,
         "hid0s": hidden_send,
-        "hid0b": lambda: hidden_block(my_z, 0),
-        "hid1": lambda: pass_on(send_hid, take_hid, 1),
-        "hid2": lambda: pass_on(send_hid, take_hid, 2),
-        "hid3": hidden_rest,
+        "hid0b": lambda: hidden_block(my_z),
+        "hid1": lambda: hidden_next(1),
+        "hid2": lambda: hidden_next(2),
+        "hid3": lambda: hidden_next(3),
         "mz0": lambda: send_mz(0),
         "mz1": lambda: pass_on(send_mz, take_mz, 1),
         "mz2": lambda: pass_on(send_mz, take_mz, 2),
         "mz3": lambda: take_mz(outer - 2),
         "proj": output_projection,
+        "fwd0": lambda: forward_hidden(0),
+        "fwd1": lambda: forward_hidden(1),
+        "fwd2": lambda: forward_hidden(2),
     }
+
+    cot_block(my_z)
 
     causal = row_id >= col_id
     causal_f = jnp.where(causal, 1.0, 0.0)
@@ -312,15 +375,6 @@
     ]
     for k in far_first:
         copy_tot[k].start()
-    copy_sl = [None] + [
-        remote(
-            slot_recv.at[my_z], slot_recv.at[my_z], sl_s.at[j], sl_r.at[j],
-            xor(my_z, j) * inner + my_q, tp,
-        )
-        for j in range(1, outer)
-    ]
-    for j in range(1, outer):
-        copy_sl[j].start()
     at("sent")
     lane = iota((1, 128), 1)
     low_lane = lane < HEAD_DIM
@@ -341,6 +395,8 @@
     def group_cols(g):
         return slice(g * gwidth, (g + 1) * gwidth)
 
+    for load in mixer_loads:
+        load.wait()
     entry_b[...] = entry[...].astype(bf16)
     for g in range(groups):
         b_g, c_g = b_in[:, tile(g)], c_in[:, tile(g)]
@@ -380,23 +436,38 @@
 
     for i in range(2, 7):
         loads[i].wait()
+    upper = my_z // per_half
+    near = upper * (outer - 1 - my_z) + (1 - upper) * my_z
+
+    def in_turn(position):
+        block = near * (1 - position) + (1 - near) * position if position < 2 else position
+        return upper * (outer - 1 - block) + (1 - upper) * block
+
+    def return_copy(peer, sem):
+        return remote(
+            ret_send.at[rowblock(peer, cap)], ret_recv.at[own_rows],
+            ret_s.at[peer], ret_r.at[sem], peer, tp,
+        )
+
     fwd_g, fwd_h, px = [], [], []
     for j in range(outer):
-        zpart = rowblock(xor(my_z, j), zrows)
+        zpart = rowblock(in_turn(j), zrows)
         fwd_g.append(
             remote(g_full.at[tp, zpart], g_full.at[tp, zpart], fg_s.at[j], fg_r.at[j], me, other)
         )
+        zpart = rowblock(xor(my_z, j), zrows)
         fwd_h.append(
             remote(h_full.at[tp, zpart], h_full.at[tp, zpart], fh_s.at[j], fh_r.at[j], me, other)
         )
         px.append(remote(part_send.at[j], part_recv.at[j], px_s.at[j], px_r.at[j], me, other))
-    for count, j in enumerate(ORDER):
-        for k in range(j * inner, (j + 1) * inner):
-            if k:
-                copy_g[k].wait_recv()
+    for j in range(outer):
+        at(("chunk", j))
+        block = in_turn(j)
+        zpart = rowblock(block, zrows)
+        for q in range(1, inner):
+            cot_copy(block, q).wait_recv()
         fwd_g[j].start()
         fwd_g[j].wait_recv()
-        zpart = rowblock(xor(my_z, j), zrows)
         act = dot_nt(g_full[0, zpart, :], wd[:, 0:half])
         act = act + dot_nt(g_full[1, zpart, :], wd[:, half:2 * half])
         gate_full = gpre[zpart, :].astype(f32)
@@ -419,10 +490,9 @@
         ret_send[zpart, :] = (own.astype(f32) + part_recv[j].astype(f32)).astype(bf16)
         if j == 0:
             ret_recv[own_rows, :] = ret_send[own_rows, :]
-        for k in range(j * inner, (j + 1) * inner):
-            if k:
-                copy_ret[k].start()
-        at(("chunk", count))
+        for q in range(inner - 1, -1, -1):
+            if j or q:
+                return_copy(block * inner + xor(my_q, q), me).start()
 
     at("experts")
 
@@ -433,20 +503,16 @@
         return carry
 
     lax.fori_loop(0, half // 256, down_step, 0)
-    stores = [
-        pltpu.make_async_copy(grad_wd.at[0], owd.at[:, 0:half], out_sem.at[0]),
-        pltpu.make_async_copy(grad_wd.at[1], owd.at[:, half:2 * half], out_sem.at[1]),
-    ]
-    stores[0].start()
-    stores[1].start()
+    store(grad_wd.at[0], owd.at[:, 0:half])
+    store(grad_wd.at[1], owd.at[:, half:2 * half])
 
     at("down")
     for k in range(1, n):
-        copy_ret[k].wait_recv()
+        return_copy(peers[k], peers[k]).wait_recv()
     moe = dot_nn(places_t[...], ret_recv[...])
     for i in range(per_half):
         cols = slice(i * dchunk, (i + 1) * dchunk)
-        hidden[tp * per_half + i] = (cot[:, cols].astype(f32) + moe[:, cols]).astype(bf16)
+        hidden[tp * per_half + i] = (cot_z[my_z, :, cols].astype(f32) + moe[:, cols]).astype(bf16)
     own_chunks = pl.ds(tp * per_half, per_half)
     copy_gh = remote(hidden.at[own_chunks], hidden.at[own_chunks], gh_s, gh_r, me, other)
     copy_gh.start()
@@ -505,6 +571,7 @@
         copy_st[k].start()
     st_recv[own_st, :] = st_send[own_st, :]
     at("states")
+    store(ogate, ogate_hbm)
 
     for g in range(groups):
         b_g, c_g = b_in[:, tile(g)], c_in[:, tile(g)]
@@ -523,6 +590,7 @@
         oc[:, tile(g)] = (gc + dot_nn(gwb, b_g)).astype(bf16)
         block_state[g] = dot_tn(gwb, c_g)
 
+    store(oc, oc_hbm)
     at("inner")
 
     for k in range(1, n):
@@ -569,6 +637,8 @@
             grad_a = jnp.where(head_l == 2 * pair, sum_low, grad_a)
             grad_a = jnp.where(head_l == 2 * pair + 1, sum_high, grad_a)
         ob[:, tile(g)] = gb.astype(bf16)
+    store(oscan, oscan_hbm)
+    store(ob, ob_hbm)
     grad_t = grad_a.T
     gat_send[...] = jnp.broadcast_to(jnp.sum(grad_t, axis=1, keepdims=True), gat_send.shape)
     copy_gat = [None] + [
@@ -579,10 +649,10 @@
         copy_gat[k].start()
     gat_recv[me] = gat_send[...]
 
+    at("final")
     for j in range(outer):
-        for copy in copy_h[j * (inner - 1):(j + 1) * (inner - 1)]:
-            copy.wait_recv()
-        fwd_h[j].start()
+        if j not in forwarded:
+            forward_hidden(j)
     for j in range(outer):
         fwd_h[j].wait_recv()
 
@@ -595,9 +665,8 @@
         return carry
 
     lax.fori_loop(0, half // 256, up_step, 0)
-    for i, (src, dst) in enumerate(((grad_wg, owg), (grad_wu, owu))):
-        stores.append(pltpu.make_async_copy(src, dst, out_sem.at[2 + i]))
-        stores[-1].start()
+    store(grad_wg, owg)
+    store(grad_wu, owu)
 
     later_sum = dot_full(grad_t, causal_f)
     for k in range(1, n):
@@ -610,18 +679,26 @@
         copy.wait_recv()
     for q in range(1, inner):
         oproj[...] += rs_recv[q].astype(f32)
+    store(oproj, proj_hbm)
     for copies in (
-        copy_g, copy_h, copy_ret, copy_st, copy_rv, copy_tot, copy_gat, copy_sl, copy_hz, fwd_z,
+        copy_st, copy_rv, copy_tot, copy_gat, copy_sl, copy_hz, fwd_z,
         copy_rs, fwd_g, fwd_h, px, [copy_gh],
     ):
         for copy in copies:
             if copy is not None:
                 copy.wait_send()
+    for b in range(outer):
+        for q in range(1, inner):
+            hidden_copy(b, q).wait_send()
+            cot_copy(b, q).wait_send()
+    for k in range(1, n):
+        return_copy(peers[k], peers[k]).wait_send()
     for s in range(outer - 1):
+        send_cot(s, drain=True)
         send_hid(s, drain=True)
         send_mz(s, drain=True)
-    for store in stores:
-        store.wait()
+    for copy in stores:
+        copy.wait()
 
 
 def pass_through(count, *refs):
@@ -681,11 +758,16 @@
     vspec = pl.BlockSpec(memory_space=pltpu.VMEM)
     aspec = pl.BlockSpec(memory_space=pl.ANY)
     scratch = [
-        vm((tokens, half), bf16), vm((outer, tokens, half), bf16),
+        vm((tokens, channels), bf16), vm((tokens, channels), bf16),
+        vm((tokens, groups * STATE), bf16), vm((tokens, groups * STATE), bf16),
+        vm((state_rows, STATE), f32), vm((dcols, channels), f32),
+        vm((tokens, channels), bf16), vm((tokens, channels), bf16),
+        vm((tokens, groups * STATE), bf16), vm((tokens, groups * STATE), bf16),
+        vm((outer, tokens, half), bf16), vm((outer, tokens, half), bf16),
         vm((rows, units), bf16), vm((rows, units), bf16),
         vm((2, half, units), bf16), vm((2, half, units), bf16),
         vm((units, width), bf16), vm((channels, width), bf16),
-        vm((rows, half), bf16), vm((outer, rows // outer, half), bf16),
+        vm((outer, rows // outer, half), bf16), vm((outer, rows // outer, half), bf16),
         vm((2, rows, half), bf16), vm((2, rows, half), bf16),
         vm((outer, rows // outer, half), bf16), vm((outer, rows // outer, half), bf16),
         vm((rows, half), bf16), vm((rows, half), bf16),
@@ -703,11 +785,11 @@
         vm((8, 128), f32), vm((n, 8, 128), f32), vm((outer, 8, tokens), f32),
         vm((heads, 128), f32), vm((n, heads, 128), f32),
         vm((2, half, units), bf16), vm((2, half, units), bf16), vm((2, units, half), bf16),
-        dma((8,)), dma((4,)),
+        dma((13,)), dma((9,)),
     ]
-    scratch += [dma((n,))] * 12
+    scratch += [dma((n,))] * 10
     scratch += [dma((outer,))] * 8
-    scratch += [dma((4, outer)), dma((4, outer)), dma((outer, inner)), dma((outer, inner))]
+    scratch += [dma((4, outer))] * 3 + [dma((outer, inner))] * 4
     scratch += [dma, dma]
     scratch += [dma((outer,))] * 4
     scratch += [dma((inner,))] * 2
@@ -719,8 +801,8 @@
             wide((tokens, channels), bf16), wide((tokens, groups * STATE), bf16),
             wide((tokens, groups * STATE), bf16), wide((heads, tokens), f32),
         ),
-        in_specs=[vspec] * 9 + [aspec] * 8,
-        out_specs=(aspec,) * 3 + (vspec,) * 6,
+        in_specs=[vspec] * 4 + [aspec] * 13,
+        out_specs=(aspec,) * 8 + (vspec,),
         scratch_shapes=scratch,
         compiler_params=pltpu.CompilerParams(
             collective_id=0, has_side_effects=True, vmem_limit_bytes=64 * 1024 * 1024 - 128 * 1024

time: 123 us -> 116 us (0.943)
  Pallas kernels: 122 us -> 115 us
    pallas_call x1, Pallas kernels: 116 us -> 109 us  [fused_body(): pl.pallas_call(functools.partial(fused, (n, outer, cap)), out_shape=(wide...]
where the time goes in v3:
time: 116 us
  Pallas kernels  115 us (99%)
    pallas_call x1, Pallas kernels, fused_body(): pl.pallas_call(functools.partial(fused, (n, outer, cap)), out_shape=(wide...  109 us
    pallas_call x1, Pallas kernels, hand_over(): pl.pallas_call(functools.partial(pass_through, count), out_shape=tuple(pi...  5.51 us

profile of v3, /device:TPU:0, one launch (start us, length us, event | category | flops | bytes accessed | tf_op | source)
XLA Modules:
  0.0 115.6 jit_solution(8570101715179222205)
XLA Ops:
  0.6 109.3 %fused.1 = (bf16[2,1024,512]{2,1,0:T(8,128)(2,1)}, bf16[2,1024,512]{2,1,0:T(8,128)(2,1)}, bf16[512,2048]{1,0:T(8,128)(2,1)}, f32[128,1024]{1,0:T(8,128)}, bf16[1...) custom-call(s32[2,128]{1,0:T(2,128)} %bitcast.22, ...), custom_call_target="tpu_custom_call" | custom-call | tf_op jit(solution)/shard_map/fused/pallas_call | solution.py:796
  109.9 5.5 %hand_over.1 = (bf16[2,1024,512]{2,1,0:T(8,128)(2,1)}, bf16[2,1024,512]{2,1,0:T(8,128)(2,1)}, bf16[512,2048]{1,0:T(8,128)(2,1)}, f32[128,1024]{1,0:T(8,128)}, bf...) custom-call(bf16[2,1024,512]{2,1,0:T(8,128)(2,1)} %get-tuple-element, ...), custom_call_target="tpu_custom_call" | custom-call | tf_op jit(solution)/shard_map/hand_over/pallas_call | solution.py:724

commit v4 on v3

--- a/solution.py
+++ b/solution.py
@@ -535,8 +535,6 @@
                 fz_s.at[j], fz_r.at[j], me, other,
             )
         )
-    for j in range(outer - 1, 0, -1):
-        copy_hz[j].start()
     at("combined")
 
     for g in range(groups):
@@ -569,6 +567,8 @@
     own_st = rowblock(me, srows)
     for k in far_first:
         copy_st[k].start()
+    for j in range(outer - 1, 0, -1):
+        copy_hz[j].start()
     st_recv[own_st, :] = st_send[own_st, :]
     at("states")
     store(ogate, ogate_hbm)

time: 116 us -> 116 us (level)
  no operation moved by 1% of the time
where the time goes in v4:
time: 116 us
  Pallas kernels  115 us (99%)
    pallas_call x1, Pallas kernels, fused_body(): pl.pallas_call(functools.partial(fused, (n, outer, cap)), out_shape=(wide...  109 us
    pallas_call x1, Pallas kernels, hand_over(): pl.pallas_call(functools.partial(pass_through, count), out_shape=tuple(pi...  5.51 us

profile of v4, /device:TPU:0, one launch (start us, length us, event | category | flops | bytes accessed | tf_op | source)
XLA Modules:
  0.0 115.6 jit_solution(16637786148300032063)
XLA Ops:
  0.6 109.3 %fused.1 = (bf16[2,1024,512]{2,1,0:T(8,128)(2,1)}, bf16[2,1024,512]{2,1,0:T(8,128)(2,1)}, bf16[512,2048]{1,0:T(8,128)(2,1)}, f32[128,1024]{1,0:T(8,128)}, bf16[1...) custom-call(s32[2,128]{1,0:T(2,128)} %bitcast.22, ...), custom_call_target="tpu_custom_call" | custom-call | tf_op jit(solution)/shard_map/fused/pallas_call | solution.py:796
  109.9 5.5 %hand_over.1 = (bf16[2,1024,512]{2,1,0:T(8,128)(2,1)}, bf16[2,1024,512]{2,1,0:T(8,128)(2,1)}, bf16[512,2048]{1,0:T(8,128)(2,1)}, f32[128,1024]{1,0:T(8,128)}, bf...) custom-call(bf16[2,1024,512]{2,1,0:T(8,128)(2,1)} %get-tuple-element, ...), custom_call_target="tpu_custom_call" | custom-call | tf_op jit(solution)/shard_map/hand_over/pallas_call | solution.py:724
